TPU v7x, 32 devices: a whole 2x2x4 slice. The times are simulated.
32 devices in a mesh: sp: 16 (over z, y, x), tp: 2 (over core).
Axes of the slice: x: 2, y: 2, z: 4, core: 2. Of those that a mesh axis runs over, the one named last changes fastest.
Arguments:
- stream: bfloat16 [4096, 2048], P('sp', 'tp'), may hold values from -80 to 80
- norm_gain: float32 [2048], P('tp'), may hold values from 0.1 to 1.9
- cotangent: bfloat16 [4096, 2048], P('sp', 'tp'), may hold values from -6 to 6
- route_weights: float32 [4096, 2], P('sp'), may hold values from 0.1 to 1.5
- routes: int32 [4096, 2], P('sp'), may hold values from 0 to 15, all different within a row; in each aligned block of 256 rows (0 to 255, 256 to 511, ...) at most 64 rows name the same one
- conv_input: bfloat16 [4096, 1024], P('sp', 'tp'), may hold values from -6 to 6
- conv_bgate: bfloat16 [4096, 1024], P('sp', 'tp'), may hold values from -6 to 6
- conv_cgate: bfloat16 [4096, 1024], P('sp', 'tp'), may hold values from -6 to 6
- conv_taps: float32 [3, 1024], P(None, 'tp'), may hold values from -3 to 3
- out_proj: bfloat16 [2048, 1024], P(None, 'tp'), may hold values from -0.1875 to 0.1875
- gate_weight: bfloat16 [16, 2048, 1024], P('sp', None, 'tp'), may hold values from -0.125 to 0.125
- up_weight: bfloat16 [16, 2048, 1024], P('sp', None, 'tp'), may hold values from -0.125 to 0.125
- down_weight: bfloat16 [16, 1024, 2048], P('sp', 'tp'), may hold values from -0.1875 to 0.1875
Outputs:
- stream_grad: bfloat16 [4096, 2048], P('sp', 'tp')
- proj_grad: float32 [2048, 1024], P('sp', 'tp')
- input_grad: bfloat16 [4096, 1024], P('sp', 'tp')
- bgate_grad: bfloat16 [4096, 1024], P('sp', 'tp')
- cgate_grad: bfloat16 [4096, 1024], P('sp', 'tp')
- gate_grad: float32 [16, 2048, 1024], P('sp', None, 'tp')
- up_grad: float32 [16, 2048, 1024], P('sp', None, 'tp')
- down_grad: float32 [16, 1024, 2048], P('sp', 'tp')
Inputs may be any that keep to these rules, and one draw needn't show every extreme that they name: `routes`: the 2 experts of a token differ. Among the tokens of one index of sp, no expert is named more than 64 times, a bound that some block reaches.
All inputs are finite; a program needn't handle non-finite values.
Results may differ from a plain program's by a relative error of at most 0.003.
The roundings to bfloat16 on the way count: a program that leaves them out, or rounds other values in their place, can miss the bound.
Values may be sent and summed in bfloat16 or wider, within the bound.
A program may use at most 128 MiB of HBM per device.

v0:
```python
import jax
import jax.numpy as jnp
from jax import lax
from jax.experimental import pallas as pl
from jax.experimental.pallas import tpu as pltpu
from jax.sharding import PartitionSpec as P

D = 2048


EPSILON = 1e-06


def shifted(value, axis, steps):
    count = lax.axis_size(axis)
    leading, last = (max(0, -steps), min(count, count - steps))
    return lax.ppermute(value, axis, [(source, source + steps) for source in range(leading, last)])


def slot_matrix(routes, experts, capacity):
    assigned = routes.reshape(-1)
    onehot = (assigned[:, None] == jnp.arange(experts, dtype=jnp.int32)[None, :]).astype(jnp.int32)
    earlier = jnp.cumsum(onehot, axis=0) - onehot
    position = jnp.sum(earlier * onehot, axis=1)
    target = assigned * capacity + position
    places = jnp.arange(experts * capacity, dtype=jnp.int32)
    return (places[:, None] == target[None, :]).astype(jnp.bfloat16)


def select_rows(selector, values):
    return jnp.dot(selector, values, preferred_element_type=jnp.float32).astype(jnp.bfloat16)


def contract_rows(left, right):
    return lax.dot_general(
        left, right, (((0,), (0,)), ((), ())), preferred_element_type=jnp.float32
    )


def contract_cols(left, right):
    return lax.dot_general(
        left, right, (((1,), (1,)), ((), ())), preferred_element_type=jnp.float32
    )


MESH = pl.DeviceIdType.MESH


def greet(count, peer_of, other=None):
    barrier = pltpu.get_barrier_semaphore()

    @pl.loop(1, count)
    def _(i):
        pl.semaphore_signal(barrier, inc=1, device_id={"sp": peer_of(i)}, device_id_type=MESH)

    if other is not None:
        pl.semaphore_signal(barrier, inc=1, device_id={"tp": other}, device_id_type=MESH)
    pl.semaphore_wait(barrier, count - 1 if other is None else count)


def dispatch_kernel(
    count,
    group,
    x_ref,
    y_ref,
    m_ref,
    ox_ref,
    oy_ref,
    om_ref,
    send,
    recv,
    fsend,
    frecv,
    msend,
    mrecv,
    own,
):
    me = lax.axis_index("sp")
    side = lax.axis_index("tp")
    other = 1 - side
    block = x_ref.shape[0] // count
    width = x_ref.shape[1]
    mine = pl.ds(pl.multiple_of(side * width, width), width)
    pairs = ((x_ref, ox_ref), (y_ref, oy_ref))

    def rows(index):
        return pl.ds(pl.multiple_of(index * block, block), block)

    def ahead(i):
        return i + side * (count - 2 * i)

    def remote(a, i):
        src, dst = pairs[a]
        peer = lax.rem(me + ahead(i), count)
        return pltpu.make_async_remote_copy(
            src_ref=src.at[rows(peer)],
            dst_ref=dst.at[rows(me), mine],
            send_sem=send.at[a, i],
            recv_sem=recv.at[a, i],
            device_id={"sp": peer},
            device_id_type=MESH,
        )

    def forward(a, i):
        dst = pairs[a][1]
        spot = dst.at[rows(lax.rem(me + count - ahead(i), count)), mine]
        return pltpu.make_async_remote_copy(
            src_ref=spot,
            dst_ref=spot,
            send_sem=fsend.at[a, i],
            recv_sem=frecv.at[a, i],
            device_id={"tp": other},
            device_id_type=MESH,
        )

    def home(a):
        src, dst = pairs[a]
        return pltpu.make_async_copy(src.at[rows(me)], dst.at[rows(me), mine], own.at[a])

    place = lax.rem(me, group)
    tokens = m_ref.shape[0]
    spot_m = om_ref.at[pl.ds(pl.multiple_of(place * tokens, tokens), tokens)]

    def mixer(i):
        return pltpu.make_async_remote_copy(
            src_ref=m_ref,
            dst_ref=spot_m,
            send_sem=msend.at[i],
            recv_sem=mrecv.at[i],
            device_id={"sp": me - place + lax.rem(place + i, group)},
            device_id_type=MESH,
        )

    home_m = pltpu.make_async_copy(m_ref, spot_m, own.at[2])
    greet(count, lambda i: lax.rem(me + i, count), other)
    for a in range(2):

        @pl.loop(1, count)
        def _(i):
            remote(a, i).start()

        home(a).start()

    @pl.loop(1, group)
    def _(i):
        mixer(i).start()

    home_m.start()
    for a in range(2):
        home(a).wait()
        forward(a, 0).start()

        @pl.loop(1, count)
        def _(i):
            remote(a, i).wait_recv()
            forward(a, i).start()

    for a in range(2):

        @pl.loop(1, count)
        def _(i):
            remote(a, i).wait_send()

        @pl.loop(0, count)
        def _(i):
            forward(a, i).wait()

    @pl.loop(1, group)
    def _(i):
        mixer(i).wait()

    home_m.wait()


def dispatch(x, y, mixed, group):
    count = lax.axis_size("sp")
    gathered = jax.ShapeDtypeStruct((group * mixed.shape[0], mixed.shape[1]), mixed.dtype)
    whole = jax.ShapeDtypeStruct((x.shape[0], 2 * x.shape[1]), x.dtype)
    return pl.pallas_call(
        lambda *refs: dispatch_kernel(count, group, *refs),
        out_shape=(whole, whole, gathered),
        in_specs=[pl.BlockSpec(memory_space=pltpu.VMEM)] * 3,
        out_specs=[pl.BlockSpec(memory_space=pltpu.VMEM)] * 3,
        scratch_shapes=[pltpu.SemaphoreType.DMA((2, count))] * 4
        + [pltpu.SemaphoreType.DMA((group,))] * 2
        + [pltpu.SemaphoreType.DMA((3,))],
        compiler_params=pltpu.CompilerParams(
            collective_id=0, has_side_effects=True, vmem_limit_bytes=40 * 2**20
        ),
        name="dispatch",
    )(x, y, mixed)


def spread_kernel(count, step, x_ref, o_ref, send, recv, own):
    me = lax.axis_index("sp")
    side = lax.axis_index("tp")
    here = lax.rem(lax.div(me, step), count)
    block = x_ref.shape[0] // count

    def rows(index):
        return pl.ds(pl.multiple_of(index * block, block), block)

    def slot(i):
        return lax.rem(here + i + side * (count - 2 * i), count)

    def peer_of(i):
        return me + (slot(i) - here) * step

    def remote(i):
        return pltpu.make_async_remote_copy(
            src_ref=x_ref.at[rows(slot(i))],
            dst_ref=o_ref.at[rows(here)],
            send_sem=send.at[i],
            recv_sem=recv.at[i],
            device_id={"sp": peer_of(i)},
            device_id_type=MESH,
        )

    greet(count, peer_of)

    @pl.loop(1, count)
    def _(i):
        remote(i).start()

    home = pltpu.make_async_copy(x_ref.at[rows(here)], o_ref.at[rows(here)], own)
    home.start()
    home.wait()

    @pl.loop(1, count)
    def _(i):
        remote(i).wait()


def spread(x, number, count, step):
    return pl.pallas_call(
        lambda *refs: spread_kernel(count, step, *refs),
        out_shape=jax.ShapeDtypeStruct(x.shape, x.dtype),
        in_specs=[pl.BlockSpec(memory_space=pltpu.VMEM)],
        out_specs=pl.BlockSpec(memory_space=pltpu.VMEM),
        scratch_shapes=[pltpu.SemaphoreType.DMA((count,))] * 2 + [pltpu.SemaphoreType.DMA],
        compiler_params=pltpu.CompilerParams(
            collective_id=number, has_side_effects=True, vmem_limit_bytes=24 * 2**20
        ),
        name="spread%d" % number,
    )(x)


def local(
    stream,
    norm_gain,
    cotangent,
    route_weights,
    routes,
    conv_input,
    conv_bgate,
    conv_cgate,
    conv_taps,
    out_proj,
    gate_weight,
    up_weight,
    down_weight,
):
    experts = lax.axis_size("sp")
    tok_count = stream.shape[0]
    top_count = routes.shape[1]
    capacity = 2 * tok_count * top_count // experts
    stream_float = stream.astype(jnp.float32)
    square_sum = lax.psum(jnp.sum(stream_float * stream_float, axis=1), "tp")
    inverse = lax.rsqrt(square_sum / D + EPSILON)[:, None]
    gain_row = norm_gain[None, :]
    normed = (stream_float * inverse * gain_row).astype(jnp.bfloat16)
    cot_float = cotangent.astype(jnp.float32)
    weighted = (route_weights[:, :, None] * cot_float[:, None, :]).astype(jnp.bfloat16)
    weighted = weighted.reshape(tok_count * top_count, -1)
    selector = slot_matrix(routes, experts, capacity)
    token_select = jnp.sum(selector.reshape(experts * capacity, tok_count, top_count), axis=2)
    send_inputs = select_rows(token_select, normed)
    send_grads = select_rows(selector, weighted)
    input_float = conv_input.astype(jnp.float32)
    cgate_float = conv_cgate.astype(jnp.float32)
    bgate_float = conv_bgate.astype(jnp.float32)
    rim_rows = shifted(jnp.stack([conv_input[-2:], conv_cgate[-2:]]), "sp", 1)
    rim_gated = rim_rows[1].astype(jnp.float32) * rim_rows[0].astype(jnp.float32)
    gated = cgate_float * input_float
    extended = jnp.concatenate([rim_gated, gated], axis=0)
    conv_out = (
        conv_taps[0][None, :] * extended[:-2]
        + conv_taps[1][None, :] * extended[1:-1]
        + conv_taps[2][None, :] * extended[2:]
    )
    mixer_out = (bgate_float * conv_out).astype(jnp.bfloat16)
    group = 2 ** ((experts.bit_length() - 1) // 2)
    stages = experts // group
    recv_inputs, recv_grads, mixer_near = dispatch(send_inputs, send_grads, mixer_out, group)
    gate_w = gate_weight[0]
    up_w = up_weight[0]
    down_w = down_weight[0]
    gate_lin = jnp.dot(recv_inputs, gate_w, preferred_element_type=jnp.float32)
    up_lin = jnp.dot(recv_inputs, up_w, preferred_element_type=jnp.float32)
    sigmoid_gate = jax.nn.sigmoid(gate_lin)
    silu_gate = gate_lin * sigmoid_gate
    hidden = (silu_gate * up_lin).astype(jnp.bfloat16)
    down_g = contract_rows(hidden, recv_grads)
    hidden_grad = contract_cols(recv_grads, down_w)
    gate_pre = (
        hidden_grad * up_lin * sigmoid_gate * (1.0 + gate_lin * (1.0 - sigmoid_gate))
    ).astype(jnp.bfloat16)
    up_pre = (hidden_grad * silu_gate).astype(jnp.bfloat16)
    gate_g = contract_rows(recv_inputs, gate_pre)
    up_g = contract_rows(recv_inputs, up_pre)
    side = lax.axis_index("tp")
    half = gate_w.shape[0] // 2

    def partial_of(part):
        gate_half = lax.dynamic_slice_in_dim(gate_w, part * half, half, axis=0)
        up_half = lax.dynamic_slice_in_dim(up_w, part * half, half, axis=0)
        value = contract_cols(gate_pre, gate_half) + contract_cols(up_pre, up_half)
        return lax.optimization_barrier(value.astype(jnp.bfloat16))

    theirs = lax.ppermute(partial_of(1 - side), "tp", [(0, 1), (1, 0)])
    summed = (partial_of(side).astype(jnp.float32) + theirs.astype(jnp.float32)).astype(
        jnp.bfloat16
    )
    returned = spread(summed, 1, experts, 1)
    normed_grad = contract_rows(token_select, returned)
    cross = lax.psum(jnp.sum(stream_float * gain_row * normed_grad, axis=1), "tp")
    stream_grad = (
        cot_float
        + inverse * gain_row * normed_grad
        - stream_float * inverse * inverse * inverse * cross[:, None] / D
    ).astype(jnp.bfloat16)
    grad_other = lax.ppermute(stream_grad, "tp", [(0, 1), (1, 0)])
    grad_whole = jnp.concatenate(
        [
            jnp.where(side == 0, stream_grad, grad_other),
            jnp.where(side == 0, grad_other, stream_grad),
        ],
        axis=1,
    )
    columns = grad_whole.reshape(tok_count, stages, group, -1).transpose(2, 0, 1, 3)
    grad_near = spread(columns.reshape(group * tok_count, -1), 2, group, 1)
    shares = contract_rows(grad_near, mixer_near).astype(jnp.bfloat16)
    shares = spread(shares, 3, stages, group)
    shares = shares.reshape(stages, shares.shape[0] // stages, -1)
    proj_grad = jnp.sum(shares.astype(jnp.float32), axis=0)
    mixer_grad = jnp.dot(grad_whole, out_proj, preferred_element_type=jnp.float32)
    delta = mixer_grad * bgate_float
    next_rim = shifted(delta[:2], "sp", -1)
    extended_back = jnp.concatenate([delta, next_rim], axis=0)
    gated_grad = (
        conv_taps[2][None, :] * extended_back[:-2]
        + conv_taps[1][None, :] * extended_back[1:-1]
        + conv_taps[0][None, :] * extended_back[2:]
    )
    bgate_grad = (mixer_grad * conv_out).astype(jnp.bfloat16)
    input_grad = (gated_grad * cgate_float).astype(jnp.bfloat16)
    cgate_grad = (gated_grad * input_float).astype(jnp.bfloat16)
    return (
        stream_grad,
        proj_grad,
        input_grad,
        bgate_grad,
        cgate_grad,
        gate_g[None],
        up_g[None],
        down_g[None],
    )


def solution(mesh):
    return jax.shard_map(
        local,
        mesh=mesh,
        in_specs=(
            P("sp", "tp"),
            P("tp"),
            P("sp", "tp"),
            P("sp", None),
            P("sp", None),
            P("sp", "tp"),
            P("sp", "tp"),
            P("sp", "tp"),
            P(None, "tp"),
            P(None, "tp"),
            P("sp", None, "tp"),
            P("sp", None, "tp"),
            P("sp", "tp", None),
        ),
        out_specs=(
            P("sp", "tp"),
            P("sp", "tp"),
            P("sp", "tp"),
            P("sp", "tp"),
            P("sp", "tp"),
            P("sp", None, "tp"),
            P("sp", None, "tp"),
            P("sp", "tp", None),
        ),
        check_vma=False,
    )
```

profile of v0, /device:TPU:17, one launch (start us, length us, event | category | flops | bytes accessed | tf_op | source)
XLA Modules:
  0.0 261.6 jit_solution(1862406260526905080)
XLA Ops:
  1.6 3.1 %collective-permute-start = (bf16[2,2,512]{2,1,0:T(2,128)(2,1)S(1)}, bf16[2,2,512]{2,1,0:T(2,128)(2,1)S(1)}, u32[]{:S(2)}, u32[]{:S(2)}) collective-permute-start(bf16[2,2,512]{2,1,0:T(2,128)(2,1)S(1)} %pad_maximum_fusion.3), channel_id=1, source_target_pairs={{0,2},{2,4},{4,6},{6,8},{8,10},{10,12},{12,14},{14,16},{16,18},{18... | collective-permute-start | bytes 12296 | tf_op jit(solution)/shard_map/ppermute | solution.py:17
  7.5 1.9 convert_multiply_fusion.4
  9.6 3.1 %psum.14 = f32[256]{0:T(256)S(1)} all-reduce(f32[256]{0:T(256)S(1)} %fusion.18), channel_id=1, replica_groups=mesh['sp'=16,'tp'=2] {'tp'}, use_global_device_ids=true, to_apply=%region_1.0 | all-reduce | flops 256 | bytes 2048 | tf_op jit(solution)/shard_map/psum | solution.py:268
  13.6 3.1 %mul.214 = f32[256,2,1024]{2,1,0:T(2,128)} broadcast(bf16[256,1024]{1,0:T(8,128)(2,1)} %param.15), dimensions={0,2} | broadcast | bytes 2621440 | tf_op jit(solution)/shard_map/mul | solution.py:273
  16.7 3.7 %mul.215 = f32[512,1024]{1,0:T(8,128)} reshape(f32[256,2,1024]{2,1,0:T(2,128)} %mul.214) | data formatting | bytes 4194304 | tf_op jit(solution)/shard_map/mul | solution.py:273
  20.3 2.1 convolution_convert_fusion.refs_0_
  22.5 2.7 %fusion.9.refs_1_ = bf16[1024,1024]{1,0:T(8,128)(2,1)} fusion(f32[512,1024]{1,0:T(8,128)S(1)} %copy-done.13, f32[512]{0:T(512)S(1)} %mul.212, s32[512]{0:T(512)S(1)} %multiply_add_fusion), kind=kOutput, calls=%fused_computation.22 | convolution fusion | flops 1076363264 | bytes 4198400 | tf_op jit(solution)/shard_map/dot_general | solution.py:31
  26.3 1.6 copy-done.2
  27.9 1.6 copy-done.3
  29.5 101.3 %dispatch.1 = (bf16[1024,2048]{1,0:T(8,128)(2,1)S(1)}, bf16[1024,2048]{1,0:T(8,128)(2,1)S(1)}, bf16[1024,512]{1,0:T(8,128)(2,1)S(1)}) custom-call(bf16[1024,1024]{1,0:T(8,128)(2,1)S(1)} %copy-done.2, bf16[1024,1024]{1,0:T(8,128)(2,1)S(1)} %copy-done.3, bf16[256,512]{1,0:T(8,128)(2,1)S(1)} %get-tuple-element.16.refs_2_), custom_call_target="tpu_custom_call" | custom-call | tf_op jit(solution)/shard_map/dispatch/pallas_call | solution.py:179
  130.8 2.3 fusion
  133.9 2.3 fusion.2
  136.2 3.0 %multiply_convert_fusion.1 = (bf16[1024,512]{1,0:T(8,128)(2,1)S(1)}, bf16[1024,512]{1,0:T(8,128)(2,1)S(1)}) fusion(f32[1024,512]{1,0:T(8,128)S(1)} %fusion, f32[1024,512]{1,0:T(8,128)S(1)} %fusion.2, bf16[1024,2048]{1,0:T(8,128)(2,1)S(1)} %get-tuple-element.11, bf16[1,512,2048]{2,1,0:T(8,128)(2,1)S(1)} %copy-done.28), kind=kOutput, calls=%fused_computation.13 | convolution fusion | flops 2154299392 | bytes 12582912 | tf_op jit(solution)/shard_map/dot_general | solution.py:41
  144.9 4.4 %convolution_bitcast_fusion.1 = f32[1,2048,512]{2,1,0:T(8,128)} fusion(bf16[1024,2048]{1,0:T(8,128)(2,1)S(1)} %get-tuple-element.12, bf16[1024,512]{1,0:T(8,128)(2,1)S(1)} %get-tuple-element.18), kind=kOutput, calls=%fused_computation.4 | convolution fusion | flops 2147483648 | bytes 9437184 | tf_op jit(solution)/shard_map/dot_general | solution.py:35
  149.3 4.7 %convolution_bitcast_fusion = f32[1,512,2048]{2,1,0:T(8,128)} fusion(bf16[1024,2048]{1,0:T(8,128)(2,1)S(1)} %get-tuple-element.11, f32[1024,512]{1,0:T(8,128)S(1)} %fusion.2, f32[1024,512]{1,0:T(8,128)S(1)} %fusion), kind=kOutput, calls=%fused_computation.3 | convolution fusion | flops 2150629376 | bytes 12582912 | tf_op jit(solution)/shard_map/dot_general | solution.py:35
  155.0 52.9 %spread1.1 = bf16[1024,1024]{1,0:T(8,128)(2,1)S(1)} custom-call(bf16[1024,1024]{1,0:T(8,128)(2,1)S(1)} %add_convert_fusion.refs_0_), custom_call_target="tpu_custom_call" | custom-call | tf_op jit(solution)/shard_map/spread1/pallas_call | solution.py:235
  208.0 1.7 fusion.20
  209.7 2.6 psum.15
  212.3 1.8 fusion.17
  214.3 6.6 %convolution_bitcast_fusion.2 = f32[1,2048,512]{2,1,0:T(8,128)} fusion(bf16[1024,2048]{1,0:T(8,128)(2,1)} %copy-done.4, bf16[1024,512]{1,0:T(8,128)(2,1)S(1)} %copy-done.9), kind=kOutput, calls=%fused_computation.5 | convolution fusion | flops 2147483648 | bytes 9437184 | tf_op jit(solution)/shard_map/dot_general | solution.py:35
  223.4 13.9 %spread2.1 = bf16[1024,512]{1,0:T(8,128)(2,1)S(1)} custom-call(bf16[1024,512]{1,0:T(8,128)(2,1)S(1)} %bitcast.83), custom_call_target="tpu_custom_call" | custom-call | tf_op jit(solution)/shard_map/spread2/pallas_call | solution.py:235
  238.1 15.8 %spread3.1 = bf16[512,512]{1,0:T(8,128)(2,1)S(1)} custom-call(bf16[512,512]{1,0:T(8,128)(2,1)S(1)} %convolution_convert_fusion.1.refs_0_), custom_call_target="tpu_custom_call" | custom-call | tf_op jit(solution)/shard_map/spread3/pallas_call | solution.py:235
  255.4 2.1 collective-permute-start.3
  258.2 1.6 collective-permute-done.3
  (102 shorter events, 20.5 us)
Async XLA Ops:
  0.6 130.1 %copy-start = (bf16[1,2048,512]{2,1,0:T(8,128)(2,1)S(1)}, bf16[1,2048,512]{2,1,0:T(8,128)(2,1)}, u32[]{:S(2)}) copy-start(bf16[1,2048,512]{2,1,0:T(8,128)(2,1)} %param.23) | copy-start | bytes 6291460
  0.6 12.1 %copy-start.25 = (s32[256,2]{0,1:T(2,128)S(1)}, s32[256,2]{0,1:T(2,128)}, u32[]{:S(2)}) copy-start(s32[256,2]{0,1:T(2,128)} %param.17) | copy-start | bytes 6148
  0.7 8.8 %copy-start.5 = (bf16[256,1024]{1,0:T(8,128)(2,1)S(1)}, bf16[256,1024]{1,0:T(8,128)(2,1)}, u32[]{:S(2)}) copy-start(bf16[256,1024]{1,0:T(8,128)(2,1)} %param.13) | copy-start | bytes 1572868
  0.7 12.1 %copy-start.27 = (f32[256,2]{0,1:T(2,128)S(1)}, f32[256,2]{0,1:T(2,128)}, u32[]{:S(2)}) copy-start(f32[256,2]{0,1:T(2,128)} %param.16) | copy-start | bytes 6148
  1.6 23.6 %collective-permute-start = (bf16[2,2,512]{2,1,0:T(2,128)(2,1)S(1)}, bf16[2,2,512]{2,1,0:T(2,128)(2,1)S(1)}, u32[]{:S(2)}, u32[]{:S(2)}) collective-permute-start(bf16[2,2,512]{2,1,0:T(2,128)(2,1)S(1)} %pad_maximum_fusion.3), channel_id=1, source_target_pairs={{0,2},{2,4},{4,6},{6,8},{8,10},{10,12},{12,14},{14,16},{16,18},{18... | collective-permute-start | bytes 12296 | tf_op jit(solution)/shard_map/ppermute | solution.py:17
  13.5 6.8 %copy-start.10 = (bf16[1024,256]{1,0:T(8,128)(2,1)}, bf16[1024,256]{1,0:T(8,128)(2,1)S(1)}, u32[]{:S(2)}) copy-start(bf16[1024,256]{1,0:T(8,128)(2,1)S(1)} %fusion.21) | copy-start | bytes 1572868
  16.7 3.7 %copy-start.24 = (f32[1024]{0:T(1024)S(1)}, f32[1024]{0:T(1024)}, u32[]{:S(2)}) copy-start(f32[1024]{0:T(1024)} %param.14) | copy-start | bytes 12292
  130.8 14.2 %copy-start.4 = (bf16[1024,2048]{1,0:T(8,128)(2,1)}, bf16[1024,2048]{1,0:T(8,128)(2,1)S(1)}, u32[]{:S(2)}) copy-start(bf16[1024,2048]{1,0:T(8,128)(2,1)S(1)} %get-tuple-element.12) | copy-start | bytes 12582916
  130.8 3.1 %copy-start.12 = (bf16[1,2048,512]{2,1,0:T(8,128)(2,1)S(1)}, bf16[1,2048,512]{2,1,0:T(8,128)(2,1)}, u32[]{:S(2)}) copy-start(bf16[1,2048,512]{2,1,0:T(8,128)(2,1)} %param.24) | copy-start | bytes 6291460
  141.9 12.2 %collective-permute-start.1 = (bf16[1024,1024]{1,0:T(8,128)(2,1)S(1)}, bf16[1024,1024]{1,0:T(8,128)(2,1)S(1)}, u32[]{:S(2)}, u32[]{:S(2)}) collective-permute-start(bf16[1024,1024]{1,0:T(8,128)(2,1)S(1)} %add_convert_fusion.1), channel_id=1, source_target_pairs={{0,1},{1,0},{2,3},{3,2},{4,5},{5,4},{6,7},{7,6},{8,9},{9,8},{10,11... | collective-permute-start | bytes 6291464 | tf_op jit(solution)/shard_map/ppermute | solution.py:320
  155.0 52.9 %copy-start.6 = (bf16[256,1024]{1,0:T(8,128)(2,1)S(1)}, bf16[256,1024]{1,0:T(8,128)(2,1)}, u32[]{:S(2)}) copy-start(bf16[256,1024]{1,0:T(8,128)(2,1)} %param.13) | copy-start | bytes 1572868
  155.0 52.9 %copy-start.11 = (bf16[1024,256]{1,0:T(8,128)(2,1)S(1)}, bf16[1024,256]{1,0:T(8,128)(2,1)}, u32[]{:S(2)}) copy-start(bf16[1024,256]{1,0:T(8,128)(2,1)} %copy-done.10) | copy-start | bytes 1572868
  208.0 4.3 %copy-start.7 = (bf16[256,1024]{1,0:T(8,128)(2,1)S(1)}, bf16[256,1024]{1,0:T(8,128)(2,1)}, u32[]{:S(2)}) copy-start(bf16[256,1024]{1,0:T(8,128)(2,1)} %param.13) | copy-start | bytes 1572868
  209.7 4.7 %copy-start.9 = (bf16[1024,512]{1,0:T(8,128)(2,1)S(1)}, bf16[1024,512]{1,0:T(8,128)(2,1)}, u32[]{:S(2)}) copy-start(bf16[1024,512]{1,0:T(8,128)(2,1)} %copy-done.8) | copy-start | bytes 3145732
  214.1 6.8 %copy-start.14 = (bf16[256,1024]{1,0:T(8,128)(2,1)}, bf16[256,1024]{1,0:T(8,128)(2,1)S(1)}, u32[]{:S(2)}) copy-start(bf16[256,1024]{1,0:T(8,128)(2,1)S(1)} %fusion.17) | copy-start | bytes 1572868
  214.1 6.8 %collective-permute-start.2 = (bf16[256,1024]{1,0:T(8,128)(2,1)S(1)}, bf16[256,1024]{1,0:T(8,128)(2,1)S(1)}, u32[]{:S(2)}, u32[]{:S(2)}) collective-permute-start(bf16[256,1024]{1,0:T(8,128)(2,1)S(1)} %fusion.17), channel_id=1, source_target_pairs={{0,1},{1,0},{2,3},{3,2},{4,5},{5,4},{6,7},{7,6},{8,9},{9,8},{10,11... | collective-permute-start | bytes 1572872 | tf_op jit(solution)/shard_map/ppermute | solution.py:332
  237.3 16.6 %copy-start.17 = (bf16[256,1024]{1,0:T(8,128)(2,1)S(1)}, bf16[256,1024]{1,0:T(8,128)(2,1)}, u32[]{:S(2)}) copy-start(bf16[256,1024]{1,0:T(8,128)(2,1)} %copy-done.16) | copy-start | bytes 1572868
  237.3 16.6 %copy-start.19 = (bf16[256,1024]{1,0:T(8,128)(2,1)S(1)}, bf16[256,1024]{1,0:T(8,128)(2,1)}, u32[]{:S(2)}) copy-start(bf16[256,1024]{1,0:T(8,128)(2,1)} %copy-done.18) | copy-start | bytes 1572868
  237.3 16.6 %copy-start.22 = (f32[256,512]{1,0:T(8,128)S(1)}, f32[256,512]{1,0:T(8,128)}, u32[]{:S(2)}) copy-start(f32[256,512]{1,0:T(8,128)} %get-tuple-element.17) | copy-start | bytes 1572868
  237.3 16.6 %copy-start.29 = (bf16[2048,512]{1,0:T(8,128)(2,1)S(1)}, bf16[2048,512]{1,0:T(8,128)(2,1)}, u32[]{:S(2)}) copy-start(bf16[2048,512]{1,0:T(8,128)(2,1)} %param.22) | copy-start | bytes 6291460
  254.0 5.9 %copy-start.20 = (bf16[256,512]{1,0:T(8,128)(2,1)S(1)}, bf16[256,512]{1,0:T(8,128)(2,1)}, u32[]{:S(2)}) copy-start(bf16[256,512]{1,0:T(8,128)(2,1)} %param.18) | copy-start | bytes 786436
  254.0 7.6 %copy-start.1 = (bf16[1,2048,512]{2,1,0:T(8,128)(2,1)S(1)}, bf16[1,2048,512]{2,1,0:T(8,128)(2,1)}, u32[]{:S(2)}) copy-start(bf16[1,2048,512]{2,1,0:T(8,128)(2,1)} %param.23) | copy-start | bytes 6291460
  255.4 5.4 %copy-start.21 = (bf16[256,512]{1,0:T(8,128)(2,1)S(1)}, bf16[256,512]{1,0:T(8,128)(2,1)}, u32[]{:S(2)}) copy-start(bf16[256,512]{1,0:T(8,128)(2,1)} %param.20) | copy-start | bytes 786436
  255.4 4.5 %collective-permute-start.3 = (f32[2,512]{1,0:T(2,128)S(1)}, f32[2,512]{1,0:T(2,128)S(1)}, u32[]{:S(2)}, u32[]{:S(2)}) collective-permute-start(f32[2,512]{1,0:T(2,128)S(1)} %slice.64), channel_id=1, source_target_pairs={{2,0},{4,2},{6,4},{8,6},{10,8},{12,10},{14,12},{16,14},{18,16},{20... | collective-permute-start | bytes 12296 | tf_op jit(solution)/shard_map/ppermute | solution.py:17
  (10 other events, 20.6 us)
where the time goes:
time: 265 us; the launch traced here: 262 us
  Pallas kernels  184 us (69%)
  matrix products  37.2 us (14%)
  local copies, waits for them, and re-layouts  15.9 us (6%)
  other arithmetic  10.3 us (4%)
  starting transfers between devices  5.85 us (2%)
  blocking collectives  5.66 us (2%)
    pallas_call x1, Pallas kernels, dispatch(): pl.pallas_call(lambda *refs: dispatch_kernel(count, group, *refs), out_sh...  101 us
    pallas_call x3, Pallas kernels, spread(): pl.pallas_call(lambda *refs: spread_kernel(count, step, *refs), out_shape...  82.6 us
    dot_general x5, matrix products, contract_rows(): lax.dot_general(left, right, (((0,), (0,)), ((), ())), preferred_element_...  18.1 us
    dot_general x5, matrix products, contract_cols(): lax.dot_general(left, right, (((1,), (1,)), ((), ())), preferred_element_...  8.2 us
    mul x3, local copies, waits for them, and re-layouts, local(): route_weights[:, :, None] * cot_float[:, None, :]  6.91 us
    unnamed x63, local copies, waits for them, and re-layouts  6.16 us
  transfers between devices with their start and end apart: 4, of which 1 were waited for; matrix products, arithmetic and copies ran while one was open for 14% of the time, Pallas kernels for 0%

commit v1 on v0

v1 whole, which is shorter than its diff:
```python
import jax
import jax.numpy as jnp
from jax import lax
from jax.experimental import pallas as pl
from jax.experimental.pallas import tpu as pltpu
from jax.sharding import PartitionSpec as P

D = 2048


EPSILON = 1e-06


def shifted(value, axis, steps):
    count = lax.axis_size(axis)
    leading, last = (max(0, -steps), min(count, count - steps))
    return lax.ppermute(value, axis, [(source, source + steps) for source in range(leading, last)])


def contract_rows(left, right):
    return lax.dot_general(
        left, right, (((0,), (0,)), ((), ())), preferred_element_type=jnp.float32
    )


def contract_cols(left, right):
    return lax.dot_general(
        left, right, (((1,), (1,)), ((), ())), preferred_element_type=jnp.float32
    )


MESH = pl.DeviceIdType.MESH


def greet(count, peer_of, other=None):
    barrier = pltpu.get_barrier_semaphore()

    @pl.loop(1, count)
    def _(i):
        pl.semaphore_signal(barrier, inc=1, device_id={"sp": peer_of(i)}, device_id_type=MESH)

    if other is not None:
        pl.semaphore_signal(barrier, inc=1, device_id={"tp": other}, device_id_type=MESH)
    pl.semaphore_wait(barrier, count - 1 if other is None else count)


def expert_kernel(
    planes,
    group,
    stream_hbm,
    gain_ref,
    cot_hbm,
    route_ref,
    u_hbm,
    b_hbm,
    c_hbm,
    taps_ref,
    gate_hbm,
    up_hbm,
    down_hbm,
    ret_ref,
    gate_out,
    up_out,
    down_out,
    slot_ref,
    inv_ref,
    conv_ref,
    near_ref,
    column,
    outgoing,
    rows_ref,
    gate_w,
    up_w,
    down_w,
    hidden_ref,
    gate_pre_ref,
    up_pre_ref,
    part_ref,
    theirs_ref,
    sum_ref,
    stream_ref,
    u_ref,
    b_ref,
    c_ref,
    rim_ref,
    mixed_ref,
    small_ref,
    square_ref,
    square_other,
    select_ref,
    scale_ref,
    load,
    hop_send,
    hop_recv,
    plane_send,
    plane_recv,
    cross_send,
    cross_recv,
    part_send,
    part_recv,
    back_send,
    back_recv,
    small_send,
    small_recv,
    rim_send,
    rim_recv,
    square_send,
    square_recv,
    mixed_send,
    mixed_recv,
):
    count = planes * group
    me = lax.axis_index("sp")
    side = lax.axis_index("tp")
    other = 1 - side
    here = lax.div(me, group)
    place = lax.rem(me, group)
    tokens = stream_ref.shape[0]
    width = column.shape[3]
    bunch = outgoing.shape[2]
    capacity = bunch // group
    f32, bf16 = jnp.float32, jnp.bfloat16

    def local(i, source, target):
        return pltpu.make_async_copy(source, target, load.at[i])

    def remote(source, target, sent, received, **peer):
        return pltpu.make_async_remote_copy(
            src_ref=source,
            dst_ref=target,
            send_sem=sent,
            recv_sem=received,
            device_id=peer,
            device_id_type=MESH,
        )

    loads = [
        local(0, cot_hbm.at[:, 0:width], column.at[here, 0]),
        local(1, cot_hbm.at[:, width : 2 * width], column.at[here, 1]),
        local(2, stream_hbm, stream_ref),
        local(3, u_hbm, u_ref),
        local(4, c_hbm, c_ref),
        local(5, b_hbm, b_ref),
        local(6, gate_hbm, gate_w),
        local(7, up_hbm, up_w),
        local(8, down_hbm, down_w),
    ]
    for copy in loads:
        copy.start()

    def hop(way, block, piece):
        spot = column.at[block, piece]
        return remote(
            spot,
            spot,
            hop_send.at[way, block, piece],
            hop_recv.at[block, piece],
            sp=me + (1 - 2 * way) * group,
        )

    def onward(way, block, piece):
        room = here < planes - 1 if way == 0 else here > 0

        @pl.when(room)
        def _():
            hop(way, block, piece).start()

    def small(i):
        return remote(
            small_ref.at[here],
            small_ref.at[here],
            small_send.at[i],
            small_recv.at[i],
            sp=lax.rem(here + i, planes) * group + place,
        )

    def small_from(i):
        return remote(
            small_ref.at[here],
            small_ref.at[lax.rem(here + planes - i, planes)],
            small_send.at[i],
            small_recv.at[i],
            sp=lax.rem(here + i, planes) * group + place,
        )

    def stripe(piece):
        return lax.div(piece, 2), 2 * side + lax.rem(piece, 2)

    def span(start, size):
        return pl.ds(pl.multiple_of(start, size), size)

    def inplane(block, piece, i):
        target = lax.rem(place + i, group)
        kind, part = stripe(piece)
        return remote(
            outgoing.at[block, piece, span(target * capacity, capacity)],
            rows_ref.at[kind, part, span(block * bunch + place * capacity, capacity)],
            plane_send.at[block, piece, i],
            plane_recv.at[block, piece, i],
            sp=here * group + target,
        )

    def cross(block, piece):
        kind, part = stripe(piece)
        spot = rows_ref.at[kind, part, span(block * bunch, bunch)]
        return remote(
            spot, spot, cross_send.at[block, piece], cross_recv.at[block, piece], tp=other
        )

    def part_copy(block, half):
        return remote(
            part_ref.at[block, :, half * width : (half + 1) * width],
            theirs_ref.at[block, :, half * width : (half + 1) * width],
            part_send.at[block, half],
            part_recv.at[block, half],
            tp=other,
        )

    def back(block, i):
        return remote(
            sum_ref.at[block, span(i * capacity, capacity)],
            ret_ref.at[span(me * capacity, capacity)],
            back_send.at[block, i],
            back_recv.at[me],
            sp=block * group + i,
        )

    def back_from(source):
        return remote(
            sum_ref.at[0, pl.ds(0, capacity)],
            ret_ref.at[span(source * capacity, capacity)],
            back_send.at[0, 0],
            back_recv.at[source],
            sp=source,
        )

    rim = rim_ref.shape[1]

    def rim_copy(i):
        source = (u_ref, c_ref)[i]
        return remote(
            source.at[tokens - rim : tokens],
            rim_ref.at[i],
            rim_send.at[i],
            rim_recv.at[i],
            sp=me + 1,
        )

    def mixed(i):
        return remote(
            mixed_ref,
            near_ref.at[span(place * tokens, tokens)],
            mixed_send.at[i],
            mixed_recv.at[i],
            sp=here * group + lax.rem(place + i, group),
        )

    square_copy = remote(square_ref, square_other, square_send, square_recv, tp=other)

    def prepare(block, way):
        wanted = lax.broadcasted_iota(jnp.int32, (bunch, tokens), 0) + here * bunch
        wanted = wanted.astype(f32)
        first = wanted == small_ref[block, 0:1, :]
        second = wanted == small_ref[block, 1:2, :]
        select_ref[way] = jnp.where(first | second, 1.0, 0.0).astype(bf16)
        weight = jnp.where(first, small_ref[block, 2:3, :], 0.0) + jnp.where(
            second, small_ref[block, 3:4, :], 0.0
        )
        scale = jnp.sum(weight, axis=1, keepdims=True)
        scale_ref[way] = jnp.broadcast_to(scale, (bunch, scale_ref.shape[2]))

    def pick(block, way, piece):
        chosen = jnp.dot(select_ref[way], column[block, piece], preferred_element_type=f32)
        scale = jnp.where(piece < 2, scale_ref[way][:, 0:1], 1.0)
        outgoing[block, piece] = (chosen * scale).astype(bf16)
        kind, part = stripe(piece)
        rows_ref[kind, part, span(block * bunch + place * capacity, capacity)] = outgoing[
            block, piece, span(place * capacity, capacity)
        ]

        @pl.loop(1, group)
        def _(i):
            inplane(block, piece, i).start()

    greet(count, lambda i: lax.rem(me + i, count), other)
    for piece in range(2):
        loads[piece].wait()
        for way in range(2):
            onward(way, here, piece)
    loads[2].wait()
    stream = stream_ref[...].astype(f32)
    lanes = square_ref.shape[1]
    total = jnp.zeros((tokens, lanes), f32)
    for start in range(0, 2 * width, lanes):
        piece_value = stream[:, start : start + lanes]
        total = total + piece_value * piece_value
    square_ref[...] = total
    square_copy.start()
    for i in range(3, 5):
        loads[i].wait()

    @pl.when(me < count - 1)
    def _():
        for i in range(2):
            rim_copy(i).start()

    @pl.when(me == 0)
    def _():
        rim_ref[...] = jnp.zeros_like(rim_ref)

    expert_row = lax.broadcasted_iota(jnp.int32, (count, tokens), 0).astype(f32)
    named = [jnp.where(expert_row == route_ref[k : k + 1, :], 1.0, 0.0) for k in range(2)]
    earlier = lax.broadcasted_iota(jnp.int32, (tokens, tokens), 0) < lax.broadcasted_iota(
        jnp.int32, (tokens, tokens), 1
    )
    before = jnp.dot(
        (named[0] + named[1]).astype(bf16),
        jnp.where(earlier, 1.0, 0.0).astype(bf16),
        preferred_element_type=f32,
    )
    slots = [
        route_ref[k : k + 1, :] * capacity + jnp.sum(named[k] * before, axis=0, keepdims=True)
        for k in range(2)
    ]
    info = jnp.concatenate(slots + [route_ref[2:8, :]], axis=0)
    small_ref[here] = info
    slot_ref[...] = info

    @pl.loop(1, planes)
    def _(i):
        small(i).start()

    prepare(here, 0)
    for piece in range(2):
        pick(here, 0, piece)
    square_copy.wait_recv()
    total = square_ref[...] + square_other[...]
    inverse = lax.rsqrt(jnp.sum(total, axis=1, keepdims=True) / (4 * width) + EPSILON)
    inv_ref[...] = jnp.broadcast_to(inverse, inv_ref.shape)
    for piece in range(2):
        cols = slice(piece * width, (piece + 1) * width)
        value = stream_ref[:, cols].astype(f32) * inverse * gain_ref[:, cols]
        column[here, 2 + piece] = value.astype(bf16)
    for piece in range(2, 4):
        for way in range(2):
            onward(way, here, piece)
    for piece in range(2, 4):
        pick(here, 0, piece)

    @pl.when(me > 0)
    def _():
        for i in range(2):
            rim_copy(i).wait_recv()

    loads[5].wait()
    gated = c_ref[...].astype(f32) * u_ref[...].astype(f32)
    rim_gated = rim_ref[1].astype(f32) * rim_ref[0].astype(f32)
    row = lax.broadcasted_iota(jnp.int32, gated.shape, 0)
    one = jnp.where(row == 0, rim_gated[rim - 1 : rim], pltpu.roll(gated, 1, 0))
    two = jnp.where(
        row == 0,
        rim_gated[rim - 2 : rim - 1],
        jnp.where(row == 1, rim_gated[rim - 1 : rim], pltpu.roll(gated, 2, 0)),
    )
    conv = taps_ref[0:1, :] * two + taps_ref[1:2, :] * one + taps_ref[2:3, :] * gated
    conv_ref[...] = conv
    mixed_value = (b_ref[...].astype(f32) * conv).astype(bf16)
    mixed_ref[...] = mixed_value
    near_ref[span(place * tokens, tokens)] = mixed_value

    @pl.loop(1, group)
    def _(i):
        mixed(i).start()

    @pl.loop(1, planes)
    def _(i):
        small_from(i).wait_recv()

    for i in range(6, 9):
        loads[i].wait()

    def arrive(step, piece):
        for way in range(2):
            block = here - step if way == 0 else here + step
            valid = (step < planes) & (block >= 0) & (block < planes)

            @pl.when(valid)
            def _():
                hop(way, block, piece).wait_recv()
                onward(way, block, piece)

        for way in range(2):
            block = here - step if way == 0 else here + step
            valid = (step < planes) & (block >= 0) & (block < planes)

            @pl.when(valid)
            def _():
                @pl.when(piece == 0)
                def _():
                    prepare(block, way)

                pick(block, way, piece)

    def gather(step, way):
        block = here - step + 2 * way * step
        valid = (block >= 0) & (block < planes) & ((way == 0) | (step > 0))

        @pl.when(valid)
        def _():
            @pl.loop(0, 4)
            def _(piece):
                @pl.loop(1, group)
                def _(i):
                    inplane(block, piece, i).wait_recv()

                cross(block, piece).start()

    def compute(step, way):
        block = here - step + 2 * way * step
        valid = (block >= 0) & (block < planes) & ((way == 0) | (step > 0))

        @pl.when(valid)
        def _():
            @pl.loop(0, 4)
            def _(piece):
                cross(block, piece).wait_recv()

            rows = span(block * bunch, bunch)
            gate_lin = jnp.zeros((bunch, gate_w.shape[1]), f32)
            up_lin = jnp.zeros((bunch, gate_w.shape[1]), f32)
            hidden_grad = jnp.zeros((bunch, gate_w.shape[1]), f32)
            for part in range(4):
                cols = slice(part * width, (part + 1) * width)
                inputs = rows_ref[1, part, rows]
                gate_lin += jnp.dot(inputs, gate_w[cols], preferred_element_type=f32)
                up_lin += jnp.dot(inputs, up_w[cols], preferred_element_type=f32)
                hidden_grad += contract_cols(rows_ref[0, part, rows], down_w[:, cols])
            sigmoid_gate = jax.nn.sigmoid(gate_lin)
            silu_gate = gate_lin * sigmoid_gate
            hidden_ref[rows] = (silu_gate * up_lin).astype(bf16)
            gate_pre = (
                hidden_grad * up_lin * sigmoid_gate * (1.0 + gate_lin * (1.0 - sigmoid_gate))
            ).astype(bf16)
            up_pre = (hidden_grad * silu_gate).astype(bf16)
            gate_pre_ref[rows] = gate_pre
            up_pre_ref[rows] = up_pre

            def partial(whose, half):
                spot = span((2 * whose + half) * width, width)
                value = contract_cols(gate_pre_ref[rows], gate_w[spot])
                value += contract_cols(up_pre_ref[rows], up_w[spot])
                return value.astype(bf16)

            for half in range(2):
                part_ref[block, :, half * width : (half + 1) * width] = partial(other, half)
                part_copy(block, half).start()
            for half in range(2):
                cols = slice(half * width, (half + 1) * width)
                mine = partial(side, half).astype(f32)
                part_copy(block, half).wait_recv()
                theirs = theirs_ref[block, :, cols].astype(f32)
                sum_ref[block, :, cols] = (mine + theirs).astype(bf16)

            @pl.loop(0, group)
            def _(i):
                @pl.when(block * group + i != me)
                def _():
                    back(block, i).start()

                @pl.when(block * group + i == me)
                def _():
                    ret_ref[span(me * capacity, capacity)] = sum_ref[
                        block, span(i * capacity, capacity)
                    ]

    @pl.loop(1, planes + 1)
    def _(step):
        arrive(step, 0)

        @pl.loop(0, 2)
        def _(way):
            gather(step - 1, way)

        @pl.loop(0, 2)
        def _(way):
            compute(step - 1, way)

        @pl.loop(1, 4)
        def _(piece):
            arrive(step, piece)

    @pl.loop(0, 4)
    def _(part):
        inputs = rows_ref[1, part]
        spot = span(part * width, width)
        gate_out[spot] = contract_rows(inputs, gate_pre_ref[...])
        up_out[spot] = contract_rows(inputs, up_pre_ref[...])
        down_out[:, spot] = contract_rows(hidden_ref[...], rows_ref[0, part])

    @pl.loop(0, count)
    def _(source):
        @pl.when(source != me)
        def _():
            back_from(source).wait_recv()

    @pl.loop(0, planes)
    def _(block):
        @pl.loop(0, 4)
        def _(piece):
            for way in range(2):
                room = here < planes - 1 if way == 0 else here > 0
                mine = block <= here if way == 0 else block >= here

                @pl.when(room & mine)
                def _():
                    hop(way, block, piece).wait_send()

            cross(block, piece).wait_send()

            @pl.loop(1, group)
            def _(i):
                inplane(block, piece, i).wait_send()

        for half in range(2):
            part_copy(block, half).wait_send()

        @pl.loop(0, group)
        def _(i):
            @pl.when(block * group + i != me)
            def _():
                back(block, i).wait_send()

    @pl.loop(1, planes)
    def _(i):
        small(i).wait_send()

    @pl.loop(1, group)
    def _(i):
        mixed(i).wait()

    @pl.when(me < count - 1)
    def _():
        for i in range(2):
            rim_copy(i).wait_send()

    square_copy.wait_send()


def experts_pass(
    group, stream, gain, cotangent, route, u, b, c, taps, gate_w, up_w, down_w
):
    count = lax.axis_size("sp")
    planes = count // group
    tokens, features = stream.shape
    width = features // 2
    channels = u.shape[1]
    hidden = gate_w.shape[1]
    capacity = 4 * tokens // count
    bunch = group * capacity
    f32, bf16 = jnp.float32, jnp.bfloat16
    shape = jax.ShapeDtypeStruct
    outs = (
        shape((count * capacity, features), bf16),
        shape(gate_w.shape, f32),
        shape(up_w.shape, f32),
        shape(down_w.shape, f32),
        shape((8, tokens), f32),
        shape((tokens, 128), f32),
        shape((tokens, channels), f32),
        shape((group * tokens, channels), bf16),
    )
    vmem, anywhere = pl.BlockSpec(memory_space=pltpu.VMEM), pl.BlockSpec(memory_space=pl.ANY)
    dma = pltpu.SemaphoreType.DMA
    return pl.pallas_call(
        lambda *refs: expert_kernel(planes, group, *refs),
        out_shape=outs,
        in_specs=[
            anywhere,
            vmem,
            anywhere,
            vmem,
            anywhere,
            anywhere,
            anywhere,
            vmem,
            anywhere,
            anywhere,
            anywhere,
        ],
        out_specs=[vmem] * 8,
        scratch_shapes=[
            pltpu.VMEM((planes, 4, tokens, width), bf16),
            pltpu.VMEM((planes, 4, bunch, width), bf16),
            pltpu.VMEM((2, 4, planes * bunch, width), bf16),
            pltpu.VMEM(gate_w.shape, bf16),
            pltpu.VMEM(up_w.shape, bf16),
            pltpu.VMEM(down_w.shape, bf16),
            pltpu.VMEM((planes * bunch, hidden), bf16),
            pltpu.VMEM((planes * bunch, hidden), bf16),
            pltpu.VMEM((planes * bunch, hidden), bf16),
            pltpu.VMEM((planes, bunch, features), bf16),
            pltpu.VMEM((planes, bunch, features), bf16),
            pltpu.VMEM((planes, bunch, features), bf16),
            pltpu.VMEM((tokens, features), bf16),
            pltpu.VMEM((tokens, channels), bf16),
            pltpu.VMEM((tokens, channels), bf16),
            pltpu.VMEM((tokens, channels), bf16),
            pltpu.VMEM((2, 16, channels), bf16),
            pltpu.VMEM((tokens, channels), bf16),
            pltpu.VMEM((planes, 8, tokens), f32),
            pltpu.VMEM((tokens, 128), f32),
            pltpu.VMEM((tokens, 128), f32),
            pltpu.VMEM((2, bunch, tokens), bf16),
            pltpu.VMEM((2, bunch, 128), f32),
            dma((9,)),
            dma((2, planes, 4)),
            dma((planes, 4)),
            dma((planes, 4, group)),
            dma((planes, 4, group)),
            dma((planes, 4)),
            dma((planes, 4)),
            dma((planes, 2)),
            dma((planes, 2)),
            dma((planes, group)),
            dma((count,)),
            dma((planes,)),
            dma((planes,)),
            dma((2,)),
            dma((2,)),
            dma,
            dma,
            dma((group,)),
            dma((group,)),
        ],
        compiler_params=pltpu.CompilerParams(
            collective_id=0, has_side_effects=True, vmem_limit_bytes=60 * 2**20
        ),
        name="experts",
    )(stream, gain, cotangent, route, u, b, c, taps, gate_w, up_w, down_w)


def spread_kernel(count, step, x_ref, o_ref, send, recv, own):
    me = lax.axis_index("sp")
    side = lax.axis_index("tp")
    here = lax.rem(lax.div(me, step), count)
    block = x_ref.shape[0] // count

    def rows(index):
        return pl.ds(pl.multiple_of(index * block, block), block)

    def slot(i):
        return lax.rem(here + i + side * (count - 2 * i), count)

    def peer_of(i):
        return me + (slot(i) - here) * step

    def remote(i):
        return pltpu.make_async_remote_copy(
            src_ref=x_ref.at[rows(slot(i))],
            dst_ref=o_ref.at[rows(here)],
            send_sem=send.at[i],
            recv_sem=recv.at[i],
            device_id={"sp": peer_of(i)},
            device_id_type=MESH,
        )

    greet(count, peer_of)

    @pl.loop(1, count)
    def _(i):
        remote(i).start()

    home = pltpu.make_async_copy(x_ref.at[rows(here)], o_ref.at[rows(here)], own)
    home.start()
    home.wait()

    @pl.loop(1, count)
    def _(i):
        remote(i).wait()


def spread(x, number, count, step):
    return pl.pallas_call(
        lambda *refs: spread_kernel(count, step, *refs),
        out_shape=jax.ShapeDtypeStruct(x.shape, x.dtype),
        in_specs=[pl.BlockSpec(memory_space=pltpu.VMEM)],
        out_specs=pl.BlockSpec(memory_space=pltpu.VMEM),
        scratch_shapes=[pltpu.SemaphoreType.DMA((count,))] * 2 + [pltpu.SemaphoreType.DMA],
        compiler_params=pltpu.CompilerParams(
            collective_id=number, has_side_effects=True, vmem_limit_bytes=24 * 2**20
        ),
        name="spread%d" % number,
    )(x)


def local(
    stream,
    norm_gain,
    cotangent,
    route_weights,
    routes,
    conv_input,
    conv_bgate,
    conv_cgate,
    conv_taps,
    out_proj,
    gate_weight,
    up_weight,
    down_weight,
):
    experts = lax.axis_size("sp")
    tok_count = stream.shape[0]
    group = 2 ** ((experts.bit_length() - 1) // 2)
    stages = experts // group
    route = jnp.concatenate(
        [
            routes.astype(jnp.float32).T,
            route_weights.T,
            jnp.zeros((4, tok_count), jnp.float32),
        ],
        axis=0,
    )
    returned, gate_g, up_g, down_g, slots, inverse, conv_out, mixer_near = experts_pass(
        group,
        stream,
        norm_gain[None, :],
        cotangent,
        route,
        conv_input,
        conv_bgate,
        conv_cgate,
        conv_taps,
        gate_weight[0],
        up_weight[0],
        down_weight[0],
    )
    side = lax.axis_index("tp")
    stream_float = stream.astype(jnp.float32)
    cot_float = cotangent.astype(jnp.float32)
    gain_row = norm_gain[None, :]
    inverse = inverse[:, 0:1]
    input_float = conv_input.astype(jnp.float32)
    cgate_float = conv_cgate.astype(jnp.float32)
    bgate_float = conv_bgate.astype(jnp.float32)
    places = jnp.arange(returned.shape[0], dtype=jnp.int32).astype(jnp.float32)[:, None]
    token_select = ((places == slots[0:1]) | (places == slots[1:2])).astype(jnp.bfloat16)
    normed_grad = contract_rows(token_select, returned)
    cross = lax.psum(jnp.sum(stream_float * gain_row * normed_grad, axis=1), "tp")
    stream_grad = (
        cot_float
        + inverse * gain_row * normed_grad
        - stream_float * inverse * inverse * inverse * cross[:, None] / D
    ).astype(jnp.bfloat16)
    grad_other = lax.ppermute(stream_grad, "tp", [(0, 1), (1, 0)])
    grad_whole = jnp.concatenate(
        [
            jnp.where(side == 0, stream_grad, grad_other),
            jnp.where(side == 0, grad_other, stream_grad),
        ],
        axis=1,
    )
    columns = grad_whole.reshape(tok_count, stages, group, -1).transpose(2, 0, 1, 3)
    grad_near = spread(columns.reshape(group * tok_count, -1), 2, group, 1)
    shares = contract_rows(grad_near, mixer_near).astype(jnp.bfloat16)
    shares = spread(shares, 3, stages, group)
    shares = shares.reshape(stages, shares.shape[0] // stages, -1)
    proj_grad = jnp.sum(shares.astype(jnp.float32), axis=0)
    mixer_grad = jnp.dot(grad_whole, out_proj, preferred_element_type=jnp.float32)
    delta = mixer_grad * bgate_float
    next_rim = shifted(delta[:2], "sp", -1)
    extended_back = jnp.concatenate([delta, next_rim], axis=0)
    gated_grad = (
        conv_taps[2][None, :] * extended_back[:-2]
        + conv_taps[1][None, :] * extended_back[1:-1]
        + conv_taps[0][None, :] * extended_back[2:]
    )
    bgate_grad = (mixer_grad * conv_out).astype(jnp.bfloat16)
    input_grad = (gated_grad * cgate_float).astype(jnp.bfloat16)
    cgate_grad = (gated_grad * input_float).astype(jnp.bfloat16)
    return (
        stream_grad,
        proj_grad,
        input_grad,
        bgate_grad,
        cgate_grad,
        gate_g[None],
        up_g[None],
        down_g[None],
    )


def solution(mesh):
    return jax.shard_map(
        local,
        mesh=mesh,
        in_specs=(
            P("sp", "tp"),
            P("tp"),
            P("sp", "tp"),
            P("sp", None),
            P("sp", None),
            P("sp", "tp"),
            P("sp", "tp"),
            P("sp", "tp"),
            P(None, "tp"),
            P(None, "tp"),
            P("sp", None, "tp"),
            P("sp", None, "tp"),
            P("sp", "tp", None),
        ),
        out_specs=(
            P("sp", "tp"),
            P("sp", "tp"),
            P("sp", "tp"),
            P("sp", "tp"),
            P("sp", "tp"),
            P("sp", None, "tp"),
            P("sp", None, "tp"),
            P("sp", "tp", None),
        ),
        check_vma=False,
    )
```

time: 265 us -> 219 us (0.83)
  matrix products: 37.2 us -> 5.73 us
  Pallas kernels: 184 us -> 175 us
  starting transfers between devices: 5.85 us -> 2.51 us
    pallas_call x3 -> x2, Pallas kernels: 82.6 us -> 53.8 us  [spread(): pl.pallas_call(lambda *refs: spread_kernel(count, step, *refs), out_shape...]
    pallas_call x1, Pallas kernels: 101 us -> 122 us  [experts_pass(): pl.pallas_call(lambda *refs: expert_kernel(planes, group, *refs), out_sha...]
    dot_general x9 -> x0, matrix products: 17.7 us -> none  [the longest x5 8.2 us: contract_cols(): lax.dot_general(left, right, (((1,), (1,)), ((), ())), preferred_element_...]
    dot_general x5 -> x2, matrix products: 18.1 us -> 4.32 us  [contract_rows(): lax.dot_general(left, right, (((0,), (0,)), ((), ())), preferred_element_...]
    mul x3 -> x0, local copies, waits for them, and re-layouts: 6.91 us -> none  [local(): route_weights[:, :, None] * cot_float[:, None, :]]
    unnamed x63 -> x38, local copies, waits for them, and re-layouts: 6.16 us -> 10.6 us
    psum x1 -> x0, blocking collectives: 3.08 us -> none  [local(): square_sum = lax.psum(jnp.sum(stream_float * stream_float, axis=1), 'tp')]
    ppermute x2 -> x1, starting transfers between devices: 5.18 us -> 2.17 us  [shifted(): lax.ppermute(value, axis, [(source, source + steps) for source in range(l...]
  transfers between devices with their start and end apart: 4 -> 2, of which waited for: 1 -> 2; matrix products, arithmetic and copies ran while one was open for 14% -> 0% of each run, Pallas kernels for 0% -> 0%
where the time goes in v1:
time: 219 us; the launch traced here: 215 us
  Pallas kernels  175 us (80%)
  local copies, waits for them, and re-layouts  14.7 us (7%)
  other arithmetic  9.36 us (4%)
  matrix products  5.73 us (3%)
  blocking collectives  3.41 us (2%)
  waiting for transfers between devices  3.29 us (2%)
  starting transfers between devices  2.51 us (1%)
    pallas_call x1, Pallas kernels, experts_pass(): pl.pallas_call(lambda *refs: expert_kernel(planes, group, *refs), out_sha...  122 us
    pallas_call x2, Pallas kernels, spread(): pl.pallas_call(lambda *refs: spread_kernel(count, step, *refs), out_shape...  53.8 us
    unnamed x38, local copies, waits for them, and re-layouts  10.6 us
  transfers between devices with their start and end apart: 2, of which 2 were waited for; matrix products, arithmetic and copies ran while one was open for 0% of the time, Pallas kernels for 0%

profile of v1, /device:TPU:17, one launch (start us, length us, event | category | flops | bytes accessed | tf_op | source)
XLA Modules:
  0.0 215.2 jit_solution(9405412061207529159)
XLA Ops:
  0.7 0.8 convert_bitcast_fusion
  1.6 1.3 maximum_maximum_fusion.refs_3_
  2.9 121.6 %experts.1 = (bf16[1024,1024]{1,0:T(8,128)(2,1)}, f32[2048,512]{1,0:T(8,128)}, f32[2048,512]{1,0:T(8,128)}, f32[512,2048]{1,0:T(8,128)}, f32[8,256]{1,0:T(8,128)...) custom-call(bf16[256,1024]{1,0:T(8,128)(2,1)} %refs_0_.1, f32[1,1024]{1,0:T(1,128)} %bitcast.36, ...), custom_call_target="tpu_custom_call" | custom-call | tf_op jit(solution)/shard_map/experts/pallas_call | solution.py:574
  124.5 1.0 slice_reduce_fusion
  125.5 0.8 fusion.23
  126.3 3.6 %fusion.7 = (f32[256]{0:T(256)S(1)}, f32[256,1024]{1,0:T(8,128)}) fusion(bf16[256,1024]{1,0:T(8,128)(2,1)S(1)} %copy-done.4, f32[1024]{0:T(1024)S(1)} %copy-done.14, bf16[1024,1024]{1,0:T(8,128)(2,1)} %get-tuple-element.18, f32[256]{0:T(256)S(1)} %bitcast.42, f32[256]{0:T(256)S(1)} %bitcast.41, f32[1024]{0:T(1024)S(1)} %iota_convert_fusion), kind=kOutput, calls=%fused_computation.10 | convolution fusion | flops 538705664 | bytes 3681280 | tf_op jit(solution)/shard_map/dot_general | solution.py:21
  129.9 3.4 %psum.7 = f32[256]{0:T(256)S(1)} all-reduce(f32[256]{0:T(256)S(1)} %get-tuple-element.35), channel_id=1, replica_groups=mesh['sp'=16,'tp'=2] {'tp'}, use_global_device_ids=true, to_apply=%region_1.0 | all-reduce | flops 256 | bytes 2048 | tf_op jit(solution)/shard_map/psum | solution.py:748
  133.3 2.5 %fusion.5 = bf16[256,1024]{1,0:T(8,128)(2,1)} fusion(bf16[256,1024]{1,0:T(8,128)(2,1)S(1)} %copy-done.4, f32[256,1024]{1,0:T(8,128)} %get-tuple-element.36, bf16[256,1024]{1,0:T(8,128)(2,1)S(1)} %copy-done.5, f32[256]{0:T(256)S(1)} %psum.7, f32[1024]{0:T(1024)S(1)} %copy-done.14, f32[256]{0:T(256)S(1)} %slice_reduce_fusion), kind=kLoop, calls=%fused_computation.8 | loop fusion | flops 3145728 | bytes 2627584 | tf_op jit(solution)/shard_map/convert_element_type | solution.py:753
  136.2 1.8 collective-permute-done
  137.9 1.2 broadcast_select_fusion.1
  140.1 1.1 pad_maximum_fusion
  141.2 1.8 reshape.31
  143.6 14.2 %spread2.1 = bf16[1024,512]{1,0:T(8,128)(2,1)S(1)} custom-call(bf16[1024,512]{1,0:T(8,128)(2,1)S(1)} %bitcast.27), custom_call_target="tpu_custom_call" | custom-call | tf_op jit(solution)/shard_map/spread2/pallas_call | solution.py:683
  158.6 39.6 %spread3.1 = bf16[512,512]{1,0:T(8,128)(2,1)S(1)} custom-call(bf16[512,512]{1,0:T(8,128)(2,1)S(1)} %convolution_convert_fusion.refs_0_), custom_call_target="tpu_custom_call" | custom-call | tf_op jit(solution)/shard_map/spread3/pallas_call | solution.py:683
  198.2 1.4 multiply_convert_fusion.1
  199.6 2.2 %collective-permute-start.1 = (f32[2,512]{1,0:T(2,128)S(1)}, f32[2,512]{1,0:T(2,128)S(1)}, u32[]{:S(2)}, u32[]{:S(2)}) collective-permute-start(f32[2,512]{1,0:T(2,128)S(1)} %slice.36), channel_id=1, source_target_pairs={{2,0},{4,2},{6,4},{8,6},{10,8},{12,10},{14,12},{16,14},{18,16},{20... | collective-permute-start | bytes 12296 | tf_op jit(solution)/shard_map/ppermute | solution.py:17
  202.6 1.5 collective-permute-done.1
  204.1 0.9 multiply_convert_fusion
  205.0 0.8 multiply_convert_fusion.2
  205.8 2.1 copy.29
  207.9 1.6 copy-done.2
  209.5 2.1 copy.30
  211.6 1.6 copy-done.1
  213.2 2.0 copy.31
  (42 shorter events, 3.5 us)
Async XLA Ops:
  0.6 197.5 %copy-start = (bf16[2048,512]{1,0:T(8,128)(2,1)S(1)}, bf16[2048,512]{1,0:T(8,128)(2,1)}, u32[]{:S(2)}) copy-start(bf16[2048,512]{1,0:T(8,128)(2,1)} %param.22) | copy-start | bytes 6291460
  2.9 123.4 %copy-start.4 = (bf16[256,1024]{1,0:T(8,128)(2,1)S(1)}, bf16[256,1024]{1,0:T(8,128)(2,1)}, u32[]{:S(2)}) copy-start(bf16[256,1024]{1,0:T(8,128)(2,1)} %refs_0_.1) | copy-start | bytes 1572868
  2.9 123.4 %copy-start.14 = (f32[1024]{0:T(1024)S(1)}, f32[1024]{0:T(1024)}, u32[]{:S(2)}) copy-start(f32[1024]{0:T(1024)} %param.14) | copy-start | bytes 12292
  126.3 7.0 %copy-start.5 = (bf16[256,1024]{1,0:T(8,128)(2,1)S(1)}, bf16[256,1024]{1,0:T(8,128)(2,1)}, u32[]{:S(2)}) copy-start(bf16[256,1024]{1,0:T(8,128)(2,1)} %refs_2_.1) | copy-start | bytes 1572868
  129.9 6.2 %copy-start.13 = (f32[3,512]{1,0:T(4,128)S(1)}, f32[3,512]{1,0:T(4,128)}, u32[]{:S(2)}) copy-start(f32[3,512]{1,0:T(4,128)} %refs_7_.1) | copy-start | bytes 18436
  135.8 2.1 collective-permute-start
  139.1 0.8 copy-start.6
  139.1 1.0 copy-start.8
  143.4 14.4 %copy-start.15 = (bf16[1024,512]{1,0:T(8,128)(2,1)S(1)}, bf16[1024,512]{1,0:T(8,128)(2,1)}, u32[]{:S(2)}) copy-start(bf16[1024,512]{1,0:T(8,128)(2,1)} %get-tuple-element.19) | copy-start | bytes 3145732
  157.8 40.4 %copy-start.7 = (bf16[256,1024]{1,0:T(8,128)(2,1)S(1)}, bf16[256,1024]{1,0:T(8,128)(2,1)}, u32[]{:S(2)}) copy-start(bf16[256,1024]{1,0:T(8,128)(2,1)} %copy-done.6) | copy-start | bytes 1572868
  157.8 40.4 %copy-start.9 = (bf16[256,1024]{1,0:T(8,128)(2,1)S(1)}, bf16[256,1024]{1,0:T(8,128)(2,1)}, u32[]{:S(2)}) copy-start(bf16[256,1024]{1,0:T(8,128)(2,1)} %copy-done.8) | copy-start | bytes 1572868
  157.8 40.4 %copy-start.12 = (bf16[256,512]{1,0:T(8,128)(2,1)S(1)}, bf16[256,512]{1,0:T(8,128)(2,1)}, u32[]{:S(2)}) copy-start(bf16[256,512]{1,0:T(8,128)(2,1)} %refs_5_.1) | copy-start | bytes 786436
  157.8 40.4 %copy-start.16 = (f32[256,512]{1,0:T(8,128)S(1)}, f32[256,512]{1,0:T(8,128)}, u32[]{:S(2)}) copy-start(f32[256,512]{1,0:T(8,128)} %get-tuple-element.20) | copy-start | bytes 1572868
  198.2 5.9 %copy-start.10 = (bf16[256,512]{1,0:T(8,128)(2,1)S(1)}, bf16[256,512]{1,0:T(8,128)(2,1)}, u32[]{:S(2)}) copy-start(bf16[256,512]{1,0:T(8,128)(2,1)} %refs_4_.1) | copy-start | bytes 786436
  198.2 7.6 %copy-start.3 = (f32[2048,512]{1,0:T(8,128)S(1)}, f32[2048,512]{1,0:T(8,128)}, u32[]{:S(2)}) copy-start(f32[2048,512]{1,0:T(8,128)} %get-tuple-element.21) | copy-start | bytes 12582916
  199.6 5.4 %copy-start.11 = (bf16[256,512]{1,0:T(8,128)(2,1)S(1)}, bf16[256,512]{1,0:T(8,128)(2,1)}, u32[]{:S(2)}) copy-start(bf16[256,512]{1,0:T(8,128)(2,1)} %refs_6_.1) | copy-start | bytes 786436
  199.6 4.5 %collective-permute-start.1 = (f32[2,512]{1,0:T(2,128)S(1)}, f32[2,512]{1,0:T(2,128)S(1)}, u32[]{:S(2)}, u32[]{:S(2)}) collective-permute-start(f32[2,512]{1,0:T(2,128)S(1)} %slice.36), channel_id=1, source_target_pairs={{2,0},{4,2},{6,4},{8,6},{10,8},{12,10},{14,12},{16,14},{18,16},{20... | collective-permute-start | bytes 12296 | tf_op jit(solution)/shard_map/ppermute | solution.py:17
  205.8 3.7 %copy-start.2 = (f32[2048,512]{1,0:T(8,128)S(1)}, f32[2048,512]{1,0:T(8,128)}, u32[]{:S(2)}) copy-start(f32[2048,512]{1,0:T(8,128)} %get-tuple-element.22) | copy-start | bytes 12582916
  209.5 3.7 %copy-start.1 = (f32[512,2048]{1,0:T(8,128)S(1)}, f32[512,2048]{1,0:T(8,128)}, u32[]{:S(2)}) copy-start(f32[512,2048]{1,0:T(8,128)} %get-tuple-element.23) | copy-start | bytes 12582916

commit v2 on v1

v2 whole, which is shorter than its diff:
```python
import jax
import jax.numpy as jnp
from jax import lax
from jax.experimental import pallas as pl
from jax.experimental.pallas import tpu as pltpu
from jax.sharding import PartitionSpec as P

EPSILON = 1e-06


def contract_rows(left, right):
    return lax.dot_general(
        left, right, (((0,), (0,)), ((), ())), preferred_element_type=jnp.float32
    )


def contract_cols(left, right):
    return lax.dot_general(
        left, right, (((1,), (1,)), ((), ())), preferred_element_type=jnp.float32
    )


MESH = pl.DeviceIdType.MESH
VMEM_LIMIT = 61 * 2**20


def layer_kernel(
    planes,
    group,
    stream_hbm,
    gain_ref,
    cot_hbm,
    weight_ref,
    route_ref,
    u_hbm,
    b_hbm,
    c_hbm,
    taps_ref,
    proj_hbm,
    gate_hbm,
    up_hbm,
    down_hbm,
    grad_hbm,
    proj_hbm_out,
    u_hbm_out,
    b_hbm_out,
    c_hbm_out,
    gate_out,
    up_out,
    down_out,
    column,
    outgoing,
    rows_ref,
    gate_w,
    up_w,
    down_w,
    hidden_ref,
    gate_pre_ref,
    up_pre_ref,
    part_ref,
    theirs_ref,
    ret_ref,
    stream_ref,
    u_ref,
    b_ref,
    c_ref,
    conv_ref,
    near_ref,
    rim_ref,
    mixed_ref,
    small_ref,
    square_ref,
    square_other,
    inner_ref,
    inner_other,
    select_ref,
    scale_ref,
    pull_ref,
    total_ref,
    grad_other,
    block_ref,
    share_ref,
    stack_ref,
    edge_ref,
    edge_next,
    grad_ref,
    proj_out,
    u_out,
    b_out,
    c_out,
    turn_ref,
    stage_ref,
    tall_ref,
    load,
    store,
    finish,
    hop_send,
    hop_recv,
    plane_send,
    plane_recv,
    cross_send,
    cross_recv,
    part_send,
    part_recv,
    back_send,
    back_recv,
    small_send,
    small_recv,
    rim_send,
    rim_recv,
    side_send,
    side_recv,
    mixed_send,
    mixed_recv,
    spread_send,
    spread_recv,
    pass_send,
    pass_recv,
    share_send,
    share_recv,
    edge_send,
    edge_recv,
):
    count = planes * group
    me = lax.axis_index("sp")
    side = lax.axis_index("tp")
    other = 1 - side
    here = lax.div(me, group)
    place = lax.rem(me, group)
    tokens = stream_ref.shape[0]
    width = column.shape[3]
    bunch = outgoing.shape[2]
    capacity = bunch // group
    f32, bf16 = jnp.float32, jnp.bfloat16

    def local(i, source, target):
        return pltpu.make_async_copy(source, target, load.at[i])

    def remote(source, target, sent, received, **peer):
        return pltpu.make_async_remote_copy(
            src_ref=source,
            dst_ref=target,
            send_sem=sent,
            recv_sem=received,
            device_id=peer,
            device_id_type=MESH,
        )

    loads = [
        local(0, cot_hbm.at[:, 0:width], column.at[here, 0]),
        local(1, cot_hbm.at[:, width : 2 * width], column.at[here, 1]),
        local(2, stream_hbm, stream_ref),
        local(3, u_hbm, u_ref),
        local(4, c_hbm, c_ref),
        local(5, b_hbm, b_ref),
        local(6, gate_hbm, gate_w),
        local(7, up_hbm, up_w),
        local(8, down_hbm, down_w),
        local(9, proj_hbm, gate_w),
    ]
    for copy in loads[:9]:
        copy.start()

    def hop(way, block, piece):
        spot = column.at[block, piece]
        return remote(
            spot,
            spot,
            hop_send.at[way, block, piece],
            hop_recv.at[block, piece],
            sp=me + (1 - 2 * way) * group,
        )

    def onward(way, block, piece):
        room = here < planes - 1 if way == 0 else here > 0

        @pl.when(room)
        def _():
            hop(way, block, piece).start()

    def small(i):
        return remote(
            small_ref.at[here],
            small_ref.at[here],
            small_send.at[i],
            small_recv.at[i],
            sp=lax.rem(here + i, planes) * group + place,
        )

    def small_from(i):
        return remote(
            small_ref.at[here],
            small_ref.at[lax.rem(here + planes - i, planes)],
            small_send.at[i],
            small_recv.at[i],
            sp=lax.rem(here + i, planes) * group + place,
        )

    def stripe(piece):
        return lax.div(piece, 2), 2 * side + lax.rem(piece, 2)

    def span(start, size):
        return pl.ds(pl.multiple_of(start, size), size)

    def inplane(block, piece, i):
        target = lax.rem(place + i, group)
        kind, part = stripe(piece)
        return remote(
            outgoing.at[block, piece, span(target * capacity, capacity)],
            rows_ref.at[kind, part, span(block * bunch + place * capacity, capacity)],
            plane_send.at[block, piece, i],
            plane_recv.at[block, piece, i],
            sp=here * group + target,
        )

    def cross(block, piece):
        kind, part = stripe(piece)
        spot = rows_ref.at[kind, part, span(block * bunch, bunch)]
        return remote(
            spot, spot, cross_send.at[block, piece], cross_recv.at[block, piece], tp=other
        )

    def part_copy(block, half):
        return remote(
            part_ref.at[block, :, half * width : (half + 1) * width],
            theirs_ref.at[block, :, half * width : (half + 1) * width],
            part_send.at[block, half],
            part_recv.at[block, half],
            tp=other,
        )

    def back(block, i):
        return remote(
            theirs_ref.at[block, span(i * capacity, capacity)],
            ret_ref.at[span(me * capacity, capacity)],
            back_send.at[block, i],
            back_recv.at[me],
            sp=block * group + i,
        )

    def back_from(source):
        return remote(
            theirs_ref.at[0, pl.ds(0, capacity)],
            ret_ref.at[span(source * capacity, capacity)],
            back_send.at[0, 0],
            back_recv.at[source],
            sp=source,
        )

    rim = rim_ref.shape[1]

    def rim_copy(i):
        source = (u_ref, c_ref)[i]
        return remote(
            source.at[tokens - rim : tokens],
            rim_ref.at[i],
            rim_send.at[i],
            rim_recv.at[i],
            sp=me + 1,
        )

    def mixed(i):
        return remote(
            mixed_ref,
            near_ref.at[span(place * tokens, tokens)],
            mixed_send.at[i],
            mixed_recv.at[i],
            sp=here * group + lax.rem(place + i, group),
        )

    def swap(i):
        mine, yours = (
            (square_ref, square_other),
            (inner_ref, inner_other),
            (grad_ref, grad_other),
        )[i]
        return remote(mine, yours, side_send.at[i], side_recv.at[i], tp=other)

    parts, sliver = block_ref.shape[0], block_ref.shape[2]
    per_part = planes // parts
    near = parts // 2
    depth = proj_out.shape[0]
    plain = per_part == 1

    def owned(part):
        return lax.div(part, near) == side

    def strip(target, part):
        if plain:
            start = ((part - side * near) * group + target) * sliver
        else:
            start = (target * near + part - side * near) * sliver
        return (grad_ref if plain else turn_ref).at[:, span(start, sliver)]

    def spread(target, part):
        return remote(
            strip(target, part),
            block_ref.at[part, span(place * tokens, tokens)],
            spread_send.at[target, part],
            spread_recv.at[place, part],
            sp=here * group + target,
        )

    def spread_from(source, part):
        return remote(
            grad_ref.at[:, pl.ds(0, sliver)],
            block_ref.at[part, span(source * tokens, tokens)],
            spread_send.at[source, part],
            spread_recv.at[source, part],
            sp=here * group + source,
        )

    def hand(part):
        spot = block_ref.at[part]
        return remote(spot, spot, pass_send.at[part], pass_recv.at[part], tp=other)

    def share(part, j):
        target = part * per_part + j
        return remote(
            share_ref.at[part, span(j * depth, depth)],
            stack_ref.at[here],
            share_send.at[part, j],
            share_recv.at[here],
            sp=target * group + place,
        )

    def share_from(source):
        return remote(
            share_ref.at[0, pl.ds(0, depth)],
            stack_ref.at[source],
            share_send.at[0, 0],
            share_recv.at[source],
            sp=source * group + place,
        )

    edge_copy = remote(edge_ref, edge_next, edge_send, edge_recv, sp=me - 1)


    def prepare(block, way):
        wanted = lax.broadcasted_iota(jnp.int32, (bunch, tokens), 0) + here * bunch
        wanted = wanted.astype(f32)
        first = wanted == small_ref[block, 0:1, :]
        second = wanted == small_ref[block, 1:2, :]
        select_ref[way] = jnp.where(first | second, 1.0, 0.0).astype(bf16)
        weight = jnp.where(first, small_ref[block, 2:3, :], 0.0) + jnp.where(
            second, small_ref[block, 3:4, :], 0.0
        )
        scale = jnp.sum(weight, axis=1, keepdims=True)
        scale_ref[way] = jnp.broadcast_to(scale, (bunch, scale_ref.shape[2]))

    def pick(block, way, piece):
        chosen = jnp.dot(select_ref[way], column[block, piece], preferred_element_type=f32)
        scale = jnp.where(piece < 2, scale_ref[way][:, 0:1], 1.0)
        outgoing[block, piece] = (chosen * scale).astype(bf16)
        kind, part = stripe(piece)
        rows_ref[kind, part, span(block * bunch + place * capacity, capacity)] = outgoing[
            block, piece, span(place * capacity, capacity)
        ]

        @pl.loop(1, group)
        def _(i):
            inplane(block, piece, i).start()

    barrier = pltpu.get_barrier_semaphore()

    @pl.loop(1, count)
    def _(i):
        pl.semaphore_signal(
            barrier, inc=1, device_id={"sp": lax.rem(me + i, count)}, device_id_type=MESH
        )

    pl.semaphore_signal(barrier, inc=1, device_id={"tp": other}, device_id_type=MESH)
    with jax.named_scope("slots"):
        names = route_ref[...].astype(f32)
        expert_row = lax.broadcasted_iota(jnp.int32, (count, tokens), 0).astype(f32)
        named = [jnp.where(expert_row == names[k : k + 1, :], 1.0, 0.0) for k in range(2)]
        earlier = lax.broadcasted_iota(jnp.int32, (tokens, tokens), 0) < lax.broadcasted_iota(
            jnp.int32, (tokens, tokens), 1
        )
        before = jnp.dot(
            (named[0] + named[1]).astype(bf16),
            jnp.where(earlier, 1.0, 0.0).astype(bf16),
            preferred_element_type=f32,
        )
        slots = [
            names[k : k + 1, :] * capacity + jnp.sum(named[k] * before, axis=0, keepdims=True)
            for k in range(2)
        ]
        info = jnp.concatenate(
            slots + [weight_ref[...], jnp.zeros((4, tokens), f32)], axis=0
        )
        small_ref[here] = info
        lanes = square_ref.shape[1]
        loads[2].wait()
        total = jnp.zeros((tokens, lanes), f32)
        for start in range(0, 2 * width, lanes):
            value = stream_ref[:, start : start + lanes].astype(f32)
            total = total + value * value
        square_ref[...] = total
        loads[0].wait()
        loads[1].wait()
    with jax.named_scope("greet"):
        pl.semaphore_wait(barrier, count)
    with jax.named_scope("own"):
        swap(0).start()

        @pl.loop(1, planes)
        def _(i):
            small(i).start()

        for i in range(3, 5):
            loads[i].wait()

        @pl.when(me < count - 1)
        def _():
            for i in range(2):
                rim_copy(i).start()

        for piece in range(2):
            for way in range(2):
                onward(way, here, piece)
        prepare(here, 0)
        for piece in range(2):
            pick(here, 0, piece)
        swap(0).wait_recv()
        total = square_ref[...] + square_other[...]
        inverse = lax.rsqrt(jnp.sum(total, axis=1, keepdims=True) / (4 * width) + EPSILON)
        for piece in range(2):
            cols = slice(piece * width, (piece + 1) * width)
            value = stream_ref[:, cols].astype(f32) * inverse * gain_ref[:, cols]
            column[here, 2 + piece] = value.astype(bf16)
        for piece in range(2, 4):
            for way in range(2):
                onward(way, here, piece)
        for piece in range(2, 4):
            pick(here, 0, piece)
        @pl.when(me == 0)
        def _():
            rim_ref[...] = jnp.zeros_like(rim_ref)

        spots = jnp.transpose(small_ref[here])
        slot = lax.broadcasted_iota(jnp.int32, pull_ref.shape, 1).astype(f32)
        hit = (slot == spots[:, 0:1]) | (slot == spots[:, 1:2])
        pull_ref[...] = jnp.where(hit, 1.0, 0.0).astype(bf16)

        @pl.loop(1, planes)
        def _(i):
            small_from(i).wait_recv()

        for i in range(5, 9):
            loads[i].wait()

    def arrive(step, piece):
        for way in range(2):
            block = here - step if way == 0 else here + step
            valid = (step < planes) & (block >= 0) & (block < planes)

            @pl.when(valid)
            def _():
                hop(way, block, piece).wait_recv()
                onward(way, block, piece)

        for way in range(2):
            block = here - step if way == 0 else here + step
            valid = (step < planes) & (block >= 0) & (block < planes)

            @pl.when(valid)
            def _():
                @pl.when(piece == 0)
                def _():
                    prepare(block, way)

                pick(block, way, piece)

    def gather(step, way):
        block = here - step + 2 * way * step
        valid = (block >= 0) & (block < planes) & ((way == 0) | (step > 0))

        @pl.when(valid)
        def _():
            @pl.loop(0, 4)
            def _(piece):
                @pl.loop(1, group)
                def _(i):
                    inplane(block, piece, i).wait_recv()

                cross(block, piece).start()

    def compute(step, way):
        block = here - step + 2 * way * step
        valid = (block >= 0) & (block < planes) & ((way == 0) | (step > 0))

        @pl.when(valid)
        def _():
            @pl.loop(0, 4)
            def _(piece):
                cross(block, piece).wait_recv()

            rows = span(block * bunch, bunch)
            gate_lin = jnp.zeros((bunch, gate_w.shape[1]), f32)
            up_lin = jnp.zeros((bunch, gate_w.shape[1]), f32)
            hidden_grad = jnp.zeros((bunch, gate_w.shape[1]), f32)
            for part in range(4):
                cols = slice(part * width, (part + 1) * width)
                inputs = rows_ref[1, part, rows]
                gate_lin += jnp.dot(inputs, gate_w[cols], preferred_element_type=f32)
                up_lin += jnp.dot(inputs, up_w[cols], preferred_element_type=f32)
                hidden_grad += contract_cols(rows_ref[0, part, rows], down_w[:, cols])
            sigmoid_gate = jax.nn.sigmoid(gate_lin)
            silu_gate = gate_lin * sigmoid_gate
            hidden_ref[rows] = (silu_gate * up_lin).astype(bf16)
            gate_pre = (
                hidden_grad * up_lin * sigmoid_gate * (1.0 + gate_lin * (1.0 - sigmoid_gate))
            ).astype(bf16)
            up_pre = (hidden_grad * silu_gate).astype(bf16)
            gate_pre_ref[rows] = gate_pre
            up_pre_ref[rows] = up_pre

            def partial(whose, half):
                spot = span((2 * whose + half) * width, width)
                value = contract_cols(gate_pre_ref[rows], gate_w[spot])
                value += contract_cols(up_pre_ref[rows], up_w[spot])
                return value.astype(bf16)

            for half in range(2):
                part_ref[block, :, half * width : (half + 1) * width] = partial(other, half)
                part_copy(block, half).start()
            for half in range(2):
                cols = slice(half * width, (half + 1) * width)
                mine = partial(side, half).astype(f32)
                part_copy(block, half).wait_recv()
                theirs = theirs_ref[block, :, cols].astype(f32)
                theirs_ref[block, :, cols] = (mine + theirs).astype(bf16)

    def written(i):
        mine, target = (
            (grad_ref, grad_hbm),
            (proj_out, proj_hbm_out),
            (u_out, u_hbm_out),
            (b_out, b_hbm_out),
            (c_out, c_hbm_out),
        )[i]
        return pltpu.make_async_copy(mine, target, finish.at[i])

    def stored(part):
        slot = lax.rem(part, 2)
        spot = span(part * width, width)
        return [
            pltpu.make_async_copy(stage_ref.at[slot, 0], gate_out.at[spot], store.at[slot, 0]),
            pltpu.make_async_copy(stage_ref.at[slot, 1], up_out.at[spot], store.at[slot, 1]),
            pltpu.make_async_copy(tall_ref.at[slot], down_out.at[:, spot], store.at[slot, 2]),
        ]

    def reply(step, way):
        block = here - step + 2 * way * step
        valid = (block >= 0) & (block < planes) & ((way == 0) | (step > 0))

        @pl.when(valid)
        def _():
            @pl.loop(0, group)
            def _(i):
                @pl.when(block * group + i != me)
                def _():
                    back(block, i).start()

                @pl.when(block * group + i == me)
                def _():
                    ret_ref[span(me * capacity, capacity)] = theirs_ref[
                        block, span(i * capacity, capacity)
                    ]

    def convolve():
        with jax.named_scope("conv"):

            @pl.when(me > 0)
            def _():
                for i in range(2):
                    rim_copy(i).wait_recv()

            gated = c_ref[...].astype(f32) * u_ref[...].astype(f32)
            rim_gated = rim_ref[1].astype(f32) * rim_ref[0].astype(f32)
            row = lax.broadcasted_iota(jnp.int32, gated.shape, 0)
            one = jnp.where(row == 0, rim_gated[rim - 1 : rim], pltpu.roll(gated, 1, 0))
            two = jnp.where(
                row == 0,
                rim_gated[rim - 2 : rim - 1],
                jnp.where(row == 1, rim_gated[rim - 1 : rim], pltpu.roll(gated, 2, 0)),
            )
            conv = taps_ref[0:1, :] * two + taps_ref[1:2, :] * one + taps_ref[2:3, :] * gated
            conv_ref[...] = conv
            mixed_value = (b_ref[...].astype(f32) * conv).astype(bf16)
            mixed_ref[...] = mixed_value
            near_ref[span(place * tokens, tokens)] = mixed_value

    inside = (here > 0) & (here < planes - 1)

    @pl.loop(1, planes + 1)
    def _(step):
        with jax.named_scope("arrive0"):

            @pl.loop(0, 2)
            def _(piece):
                arrive(step, piece)

        with jax.named_scope("gather"):

            @pl.loop(0, 2)
            def _(way):
                gather(step - 1, way)

        @pl.loop(0, 2)
        def _(way):
            with jax.named_scope("compute"):
                compute(step - 1, way)

        with jax.named_scope("arrive2"):

            @pl.loop(2, 4)
            def _(piece):
                arrive(step, piece)

        @pl.loop(0, 2)
        def _(way):
            reply(step - 1, way)

        @pl.when(step == 1)
        def _():
            convolve()

        @pl.when(step == jnp.where(inside, planes, 2))
        def _():
            @pl.loop(1, group)
            def _(i):
                mixed(i).start()

    loads[9].start()
    with jax.named_scope("wgrad"):

        @pl.loop(0, 4)
        def _(part):
            slot = lax.rem(part, 2)

            @pl.when(part >= 2)
            def _():
                for copy in stored(part - 2):
                    copy.wait()

            inputs = rows_ref[1, part]
            stage_ref[slot, 0] = contract_rows(inputs, gate_pre_ref[...])
            stage_ref[slot, 1] = contract_rows(inputs, up_pre_ref[...])
            tall_ref[slot] = contract_rows(hidden_ref[...], rows_ref[0, part])
            for copy in stored(part):
                copy.start()

    @pl.loop(0, planes)
    def _(turn):
        block = lax.rem(here + turn, planes)
        with jax.named_scope("returned"):

            @pl.loop(0, group)
            def _(i):
                @pl.when(block * group + i != me)
                def _():
                    back_from(block * group + i).wait_recv()

        with jax.named_scope("pull"):
            rows = span(block * bunch, bunch)
            value = jnp.dot(pull_ref[:, rows], ret_ref[rows], preferred_element_type=f32)

            @pl.when(turn == 0)
            def _():
                total_ref[...] = value

            @pl.when(turn > 0)
            def _():
                total_ref[...] += value

    with jax.named_scope("cross"):
        total = jnp.zeros((tokens, lanes), f32)
        for start in range(0, 2 * width, lanes):
            cols = slice(start, start + lanes)
            total += stream_ref[:, cols].astype(f32) * gain_ref[:, cols] * total_ref[:, cols]
        inner_ref[...] = total
        swap(1).start()
        square = jnp.sum(square_ref[...] + square_other[...], axis=1, keepdims=True)
        inverse = lax.rsqrt(square / (4 * width) + EPSILON)
        swap(1).wait_recv()
        inner = jnp.sum(inner_ref[...] + inner_other[...], axis=1, keepdims=True)
        pull_back = inverse * inverse * inverse * inner / (4 * width)
        for piece in range(2):
            cols = slice(piece * width, (piece + 1) * width)
            grad_ref[:, cols] = (
                column[here, piece].astype(f32)
                + inverse * gain_ref[:, cols] * total_ref[:, cols]
                - stream_ref[:, cols].astype(f32) * pull_back
            ).astype(bf16)
        swap(2).start()
        written(0).start()

    upper = here >= planes // 2
    base = lax.div(here * parts, planes)

    def turned(k):
        return lax.rem(base + parts + jnp.where(upper, 1 + k, parts - 1 - k), parts)

    with jax.named_scope("spread"):

        if not plain:
            features = 2 * width
            run = near * sliver
            for start in range(0, features, sliver):
                goal = lax.broadcasted_iota(jnp.int32, (features, sliver), 1) + start
                inner_goal = lax.rem(goal, run)
                origin = (
                    lax.div(inner_goal, depth) * group + lax.div(goal, run)
                ) * depth + lax.rem(inner_goal, depth)
                match = lax.broadcasted_iota(jnp.int32, (features, sliver), 0) == origin
                turn_ref[:, start : start + sliver] = jnp.dot(
                    grad_ref[...],
                    jnp.where(match, 1.0, 0.0).astype(bf16),
                    preferred_element_type=f32,
                ).astype(bf16)

        @pl.loop(0, parts)
        def _(k):
            part = turned(k)

            @pl.when(owned(part))
            def _():
                @pl.loop(0, group)
                def _(target):
                    @pl.when(target != place)
                    def _():
                        spread(target, part).start()

                block_ref[part, span(place * tokens, tokens)] = strip(place, part)[...]

    with jax.named_scope("mixer"):
        half = 2 * width
        loads[9].wait()
        mixer_grad = jnp.dot(
            grad_ref[...], gate_w[span(side * half, half)], preferred_element_type=f32
        )
        swap(2).wait_recv()
        mixer_grad += jnp.dot(
            grad_other[...], gate_w[span(other * half, half)], preferred_element_type=f32
        )
        delta = mixer_grad * b_ref[...].astype(f32)
        edge_ref[...] = delta[0 : edge_ref.shape[0]]

        @pl.when(me > 0)
        def _():
            edge_copy.start()

        b_out[...] = (mixer_grad * conv_ref[...]).astype(bf16)
        written(3).start()

    @pl.loop(1, group)
    def _(i):
        mixed(i).wait()

    @pl.loop(0, parts)
    def _(k):
        part = turned(k)
        with jax.named_scope("collect"):

            @pl.when(owned(part))
            def _():
                @pl.loop(0, group)
                def _(source):
                    @pl.when(source != place)
                    def _():
                        spread_from(source, part).wait_recv()

                hand(part).start()

            @pl.when(jnp.logical_not(owned(part)))
            def _():
                hand(part).wait_recv()

        with jax.named_scope("shares"):
            value = contract_rows(block_ref[part], near_ref[...])
            share_ref[part] = value.astype(bf16)
            for j in range(per_part):

                @pl.when(part * per_part + j != here)
                def _():
                    share(part, j).start()

                @pl.when(part * per_part + j == here)
                def _():
                    proj_out[...] = value[j * depth : (j + 1) * depth]

    with jax.named_scope("edge"):

        @pl.when(me == count - 1)
        def _():
            edge_next[...] = jnp.zeros_like(edge_next)

        @pl.when(me < count - 1)
        def _():
            edge_copy.wait_recv()

        row = lax.broadcasted_iota(jnp.int32, delta.shape, 0)
        one = jnp.where(
            row == tokens - 1, edge_next[0:1], pltpu.roll(delta, tokens - 1, 0)
        )
        two = jnp.where(
            row == tokens - 2,
            edge_next[0:1],
            jnp.where(row == tokens - 1, edge_next[1:2], pltpu.roll(delta, tokens - 2, 0)),
        )
        gated_grad = taps_ref[2:3, :] * delta + taps_ref[1:2, :] * one + taps_ref[0:1, :] * two
        u_out[...] = (gated_grad * c_ref[...].astype(f32)).astype(bf16)
        c_out[...] = (gated_grad * u_ref[...].astype(f32)).astype(bf16)
        written(2).start()
        written(4).start()

    for part in range(2, 4):
        for copy in stored(part):
            copy.wait()

    with jax.named_scope("final"):

        @pl.loop(1, planes)
        def _(i):
            source = lax.rem(here + i, planes)
            share_from(source).wait_recv()
            proj_out[...] += stack_ref[source].astype(f32)

    written(1).start()

    @pl.loop(0, planes)
    def _(block):
        @pl.loop(0, 4)
        def _(piece):
            for way in range(2):
                room = here < planes - 1 if way == 0 else here > 0
                mine = block <= here if way == 0 else block >= here

                @pl.when(room & mine)
                def _():
                    hop(way, block, piece).wait_send()

            cross(block, piece).wait_send()

            @pl.loop(1, group)
            def _(i):
                inplane(block, piece, i).wait_send()

        for half in range(2):
            part_copy(block, half).wait_send()

        @pl.loop(0, group)
        def _(i):
            @pl.when(block * group + i != me)
            def _():
                back(block, i).wait_send()

    @pl.loop(1, planes)
    def _(i):
        small(i).wait_send()

    @pl.when(me < count - 1)
    def _():
        for i in range(2):
            rim_copy(i).wait_send()

    @pl.when(me > 0)
    def _():
        edge_copy.wait_send()

    for i in range(3):
        swap(i).wait_send()

    @pl.loop(0, parts)
    def _(part):
        @pl.when(owned(part))
        def _():
            @pl.loop(0, group)
            def _(target):
                @pl.when(target != place)
                def _():
                    spread(target, part).wait_send()

            hand(part).wait_send()

        for j in range(per_part):

            @pl.when(part * per_part + j != here)
            def _():
                share(part, j).wait_send()

    for i in range(5):
        written(i).wait()


def local(
    stream,
    norm_gain,
    cotangent,
    route_weights,
    routes,
    conv_input,
    conv_bgate,
    conv_cgate,
    conv_taps,
    out_proj,
    gate_weight,
    up_weight,
    down_weight,
):
    count = lax.axis_size("sp")
    group = 2 ** ((count.bit_length() - 1) // 2)
    planes = count // group
    tokens, features = stream.shape
    width = features // 2
    channels = conv_input.shape[1]
    gate_shape, down_shape = gate_weight.shape[1:], down_weight.shape[1:]
    hidden = gate_shape[1]
    capacity = 2 * tokens * routes.shape[1] // count
    bunch = group * capacity
    slots = count * capacity
    depth = 2 * features // count
    sliver = max(128, depth)
    parts = planes * depth // sliver
    f32, bf16 = jnp.float32, jnp.bfloat16
    shape = jax.ShapeDtypeStruct
    outs = (
        shape(stream.shape, bf16),
        shape((depth, channels), f32),
        shape(conv_input.shape, bf16),
        shape(conv_input.shape, bf16),
        shape(conv_input.shape, bf16),
        shape(gate_shape, f32),
        shape(gate_shape, f32),
        shape(down_shape, f32),
    )
    vmem, hbm = pl.BlockSpec(memory_space=pltpu.VMEM), pl.BlockSpec(memory_space=pltpu.HBM)
    dma = pltpu.SemaphoreType.DMA
    results = pl.pallas_call(
        lambda *refs: layer_kernel(planes, group, *refs),
        out_shape=outs,
        in_specs=[hbm, vmem, hbm, vmem, vmem, hbm, hbm, hbm, vmem, hbm, hbm, hbm, hbm],
        out_specs=[hbm] * 8,
        scratch_shapes=[
            pltpu.VMEM((planes, 4, tokens, width), bf16),
            pltpu.VMEM((planes, 4, bunch, width), bf16),
            pltpu.VMEM((2, 4, slots, width), bf16),
            pltpu.VMEM(gate_shape, bf16),
            pltpu.VMEM(gate_shape, bf16),
            pltpu.VMEM(down_shape, bf16),
            pltpu.VMEM((slots, hidden), bf16),
            pltpu.VMEM((slots, hidden), bf16),
            pltpu.VMEM((slots, hidden), bf16),
            pltpu.VMEM((planes, bunch, features), bf16),
            pltpu.VMEM((planes, bunch, features), bf16),
            pltpu.VMEM((slots, features), bf16),
            pltpu.VMEM((tokens, features), bf16),
            pltpu.VMEM((tokens, channels), bf16),
            pltpu.VMEM((tokens, channels), bf16),
            pltpu.VMEM((tokens, channels), bf16),
            pltpu.VMEM((tokens, channels), f32),
            pltpu.VMEM((group * tokens, channels), bf16),
            pltpu.VMEM((2, 16, channels), bf16),
            pltpu.VMEM((tokens, channels), bf16),
            pltpu.VMEM((planes, 8, tokens), f32),
            pltpu.VMEM((tokens, 128), f32),
            pltpu.VMEM((tokens, 128), f32),
            pltpu.VMEM((tokens, 128), f32),
            pltpu.VMEM((tokens, 128), f32),
            pltpu.VMEM((2, bunch, tokens), bf16),
            pltpu.VMEM((2, bunch, 128), f32),
            pltpu.VMEM((tokens, slots), bf16),
            pltpu.VMEM((tokens, features), f32),
            pltpu.VMEM((tokens, features), bf16),
            pltpu.VMEM((parts, group * tokens, sliver), bf16),
            pltpu.VMEM((parts, sliver, channels), bf16),
            pltpu.VMEM((planes, depth, channels), bf16),
            pltpu.VMEM((8, channels), f32),
            pltpu.VMEM((8, channels), f32),
            pltpu.VMEM(stream.shape, bf16),
            pltpu.VMEM((depth, channels), f32),
            pltpu.VMEM(conv_input.shape, bf16),
            pltpu.VMEM(conv_input.shape, bf16),
            pltpu.VMEM(conv_input.shape, bf16),
            pltpu.VMEM(stream.shape if sliver > depth else (8, 128), bf16),
            pltpu.VMEM((2, 2, width, hidden), f32),
            pltpu.VMEM((2, hidden, width), f32),
            dma((10,)),
            dma((2, 3)),
            dma((5,)),
            dma((2, planes, 4)),
            dma((planes, 4)),
            dma((planes, 4, group)),
            dma((planes, 4, group)),
            dma((planes, 4)),
            dma((planes, 4)),
            dma((planes, 2)),
            dma((planes, 2)),
            dma((planes, group)),
            dma((count,)),
            dma((planes,)),
            dma((planes,)),
            dma((2,)),
            dma((2,)),
            dma((3,)),
            dma((3,)),
            dma((group,)),
            dma((group,)),
            dma((group, parts)),
            dma((group, parts)),
            dma((parts,)),
            dma((parts,)),
            dma((parts, planes // parts)),
            dma((planes,)),
            dma,
            dma,
        ],
        compiler_params=pltpu.CompilerParams(
            collective_id=0, has_side_effects=True, vmem_limit_bytes=VMEM_LIMIT
        ),
        name="layer",
    )(
        stream,
        norm_gain[None, :],
        cotangent,
        route_weights.T,
        routes.T,
        conv_input,
        conv_bgate,
        conv_cgate,
        conv_taps,
        out_proj,
        gate_weight[0],
        up_weight[0],
        down_weight[0],
    )
    return results[:5] + tuple(value[None] for value in results[5:])


def solution(mesh):
    return jax.shard_map(
        local,
        mesh=mesh,
        in_specs=(
            P("sp", "tp"),
            P("tp"),
            P("sp", "tp"),
            P("sp", None),
            P("sp", None),
            P("sp", "tp"),
            P("sp", "tp"),
            P("sp", "tp"),
            P(None, "tp"),
            P(None, "tp"),
            P("sp", None, "tp"),
            P("sp", None, "tp"),
            P("sp", "tp", None),
        ),
        out_specs=(
            P("sp", "tp"),
            P("sp", "tp"),
            P("sp", "tp"),
            P("sp", "tp"),
            P("sp", "tp"),
            P("sp", None, "tp"),
            P("sp", None, "tp"),
            P("sp", "tp", None),
        ),
        check_vma=False,
    )
```

time: 219 us -> 158 us (0.72); the launches traced: 215 us -> 157 us
  Pallas kernels: 175 us -> 137 us
  other arithmetic: 9.36 us -> 0 us
  matrix products: 5.73 us -> 0 us
  local copies, waits for them, and re-layouts: 14.7 us -> 19.1 us
  blocking collectives: 3.41 us -> 0 us
  waiting for transfers between devices: 3.29 us -> 0 us
  starting transfers between devices: 2.51 us -> 0 us
    pallas_call x3 -> x1, Pallas kernels: 175 us -> 137 us  [local(): pl.pallas_call(lambda *refs: layer_kernel(planes, group, *refs), out_shap...]
    unnamed x38 -> x12, local copies, waits for them, and re-layouts: 10.6 us -> 19.1 us
    dot_general x3 -> x0, matrix products: 5.73 us -> none  [the longest x2 4.32 us: contract_rows(): lax.dot_general(left, right, (((0,), (0,)), ((), ())), preferred_element_...]
    convert_element_type x4 -> x0, other arithmetic: 4.18 us -> none  [the longest x1 2.49 us: local(): stream_grad = (cot_float + inverse * gain_row * normed_grad - stream_floa...]
    psum x1 -> x0, blocking collectives: 3.41 us -> none  [local(): lax.psum(jnp.sum(stream_float * gain_row * normed_grad, axis=1), 'tp')]
    ppermute x2 -> x0, waiting for transfers between devices: 3.29 us -> none  [the longest x1 1.77 us: local(): grad_other = lax.ppermute(stream_grad, 'tp', [(0, 1), (1, 0)])]
    ppermute x2 -> x0, starting transfers between devices: 2.51 us -> none  [the longest x1 2.17 us: shifted(): lax.ppermute(value, axis, [(source, source + steps) for source in range(l...]
    concatenate x2 -> x0, other arithmetic: 2.4 us -> none  [the longest x1 1.35 us: local(): jnp.concatenate([routes.astype(jnp.float32).T, route_weights.T, jnp.zeros...]
  transfers between devices with their start and end apart: 2 -> 0, of which waited for: 2 -> 0; matrix products, arithmetic and copies ran while one was open for 0% -> 0% of each run, Pallas kernels for 0% -> 0%
where the time goes in v2:
time: 158 us; the launch traced here: 157 us
  Pallas kernels  137 us (87%)
  local copies, waits for them, and re-layouts  19.1 us (12%)
    pallas_call x1, Pallas kernels, local(): pl.pallas_call(lambda *refs: layer_kernel(planes, group, *refs), out_shap...  137 us
    unnamed x12, local copies, waits for them, and re-layouts  19.1 us

profile of v2, /device:TPU:17, one launch (start us, length us, event | category | flops | bytes accessed | tf_op | source)
XLA Modules:
  0.0 157.0 jit_solution(9657780548685544190)
XLA Ops:
  0.6 137.3 %layer.1 = (bf16[256,1024]{1,0:T(8,128)(2,1)}, f32[128,512]{1,0:T(8,128)}, bf16[256,512]{1,0:T(8,128)(2,1)}, bf16[256,512]{1,0:T(8,128)(2,1)}, bf16[256,512]{1,0...) custom-call(bf16[256,1024]{1,0:T(8,128)(2,1)} %refs_0_.1, f32[1,1024]{1,0:T(1,128)} %bitcast.15, ...), custom_call_target="tpu_custom_call" | custom-call | tf_op jit(solution)/shard_map/layer/pallas_call | solution.py:941
  137.9 1.9 %copy.29 = bf16[256,1024]{1,0:T(8,128)(2,1)} copy(bf16[256,1024]{1,0:T(8,128)(2,1)} %get-tuple-element.32) | data formatting | bytes 1048576
  139.8 1.7 %copy.30 = f32[128,512]{1,0:T(8,128)} copy(f32[128,512]{1,0:T(8,128)} %get-tuple-element.33) | data formatting | bytes 524288
  141.4 1.7 %copy.31 = bf16[256,512]{1,0:T(8,128)(2,1)} copy(bf16[256,512]{1,0:T(8,128)(2,1)} %get-tuple-element.34) | data formatting | bytes 524288
  143.1 1.7 %copy.32 = bf16[256,512]{1,0:T(8,128)(2,1)} copy(bf16[256,512]{1,0:T(8,128)(2,1)} %get-tuple-element.35) | data formatting | bytes 524288
  144.8 1.7 %copy.33 = bf16[256,512]{1,0:T(8,128)(2,1)} copy(bf16[256,512]{1,0:T(8,128)(2,1)} %get-tuple-element.36) | data formatting | bytes 524288
  146.5 0.0 copy-start.1
  146.5 4.8 %copy.34 = f32[1,2048,512]{2,1,0:T(8,128)} copy(f32[1,2048,512]{2,1,0:T(8,128)} %bitcast.11) | data formatting | bytes 8388608
  151.3 0.0 copy-done.1
  151.3 0.0 copy-start
  151.3 2.1 %copy.35 = f32[1,2048,512]{2,1,0:T(8,128)} copy(f32[1,2048,512]{2,1,0:T(8,128)S(1)} %bitcast.10) | data formatting | bytes 8388608
  153.4 1.6 copy-done
  155.0 2.0 %copy.36 = f32[1,512,2048]{2,1,0:T(8,128)} copy(f32[1,512,2048]{2,1,0:T(8,128)S(1)} %bitcast.9) | data formatting | bytes 8388608
Async XLA Ops:
  146.5 4.8 %copy-start.1 = (f32[2048,512]{1,0:T(8,128)S(1)}, f32[2048,512]{1,0:T(8,128)}, u32[]{:S(2)}) copy-start(f32[2048,512]{1,0:T(8,128)} %get-tuple-element.22) | copy-start | bytes 12582916
  151.3 3.7 %copy-start = (f32[512,2048]{1,0:T(8,128)S(1)}, f32[512,2048]{1,0:T(8,128)}, u32[]{:S(2)}) copy-start(f32[512,2048]{1,0:T(8,128)} %get-tuple-element.23) | copy-start | bytes 12582916

commit v3 on v2

--- a/solution.py
+++ b/solution.py
@@ -21,113 +21,104 @@
 
 
 MESH = pl.DeviceIdType.MESH
-VMEM_LIMIT = 61 * 2**20
+MIB = 2**20
 
 
 def layer_kernel(
     planes,
     group,
     stream_hbm,
-    gain_ref,
+    gain_hbm,
     cot_hbm,
-    weight_ref,
-    route_ref,
+    weight_hbm,
+    route_hbm,
     u_hbm,
     b_hbm,
     c_hbm,
-    taps_ref,
+    taps_hbm,
     proj_hbm,
     gate_hbm,
     up_hbm,
     down_hbm,
-    grad_hbm,
-    proj_hbm_out,
-    u_hbm_out,
-    b_hbm_out,
-    c_hbm_out,
-    gate_out,
-    up_out,
-    down_out,
-    column,
-    outgoing,
-    rows_ref,
-    gate_w,
-    up_w,
-    down_w,
-    hidden_ref,
-    gate_pre_ref,
-    up_pre_ref,
-    part_ref,
-    theirs_ref,
-    ret_ref,
-    stream_ref,
-    u_ref,
-    b_ref,
-    c_ref,
-    conv_ref,
-    near_ref,
-    rim_ref,
-    mixed_ref,
-    small_ref,
-    square_ref,
-    square_other,
-    inner_ref,
-    inner_other,
-    select_ref,
-    scale_ref,
-    pull_ref,
-    total_ref,
-    grad_other,
-    block_ref,
-    share_ref,
-    stack_ref,
-    edge_ref,
-    edge_next,
     grad_ref,
     proj_out,
     u_out,
     b_out,
     c_out,
-    turn_ref,
-    stage_ref,
-    tall_ref,
-    load,
-    store,
-    finish,
-    hop_send,
-    hop_recv,
-    plane_send,
-    plane_recv,
-    cross_send,
-    cross_recv,
-    part_send,
-    part_recv,
-    back_send,
-    back_recv,
-    small_send,
-    small_recv,
-    rim_send,
-    rim_recv,
-    side_send,
-    side_recv,
-    mixed_send,
-    mixed_recv,
-    spread_send,
-    spread_recv,
-    pass_send,
-    pass_recv,
-    share_send,
-    share_recv,
-    edge_send,
-    edge_recv,
+    *rest,
 ):
+    pieces = rest[:12]
+    (
+        gain_ref,
+        weight_ref,
+        route_ref,
+        taps_ref,
+        column,
+        outgoing,
+        rows_ref,
+        gate_w,
+        up_w,
+        down_w,
+        hidden_ref,
+        gate_pre_ref,
+        up_pre_ref,
+        part_ref,
+        theirs_ref,
+        ret_ref,
+            u_ref,
+        b_ref,
+        c_ref,
+            near_ref,
+        rim_ref,
+        small_ref,
+        square_ref,
+        square_other,
+        inner_ref,
+        inner_other,
+        select_ref,
+            spots_ref,
+        total_ref,
+        grad_other,
+        block_ref,
+            stack_ref,
+        edge_ref,
+        edge_next,
+        turn_ref,
+        load,
+        hop_send,
+        hop_recv,
+        plane_send,
+        plane_recv,
+        cross_send,
+        cross_recv,
+        part_send,
+        part_recv,
+        back_send,
+        back_recv,
+        small_send,
+        small_recv,
+        rim_send,
+        rim_recv,
+        side_send,
+        side_recv,
+        mixed_send,
+        mixed_recv,
+        spread_send,
+        spread_recv,
+        pass_send,
+        pass_recv,
+        share_send,
+        share_recv,
+        edge_send,
+        edge_recv,
+    ) = rest[12:]
     count = planes * group
     me = lax.axis_index("sp")
     side = lax.axis_index("tp")
     other = 1 - side
     here = lax.div(me, group)
     place = lax.rem(me, group)
-    tokens = stream_ref.shape[0]
+    tokens = grad_ref.shape[0]
     width = column.shape[3]
     bunch = outgoing.shape[2]
     capacity = bunch // group
@@ -147,18 +138,22 @@
         )
 
     loads = [
-        local(0, cot_hbm.at[:, 0:width], column.at[here, 0]),
-        local(1, cot_hbm.at[:, width : 2 * width], column.at[here, 1]),
-        local(2, stream_hbm, stream_ref),
-        local(3, u_hbm, u_ref),
-        local(4, c_hbm, c_ref),
-        local(5, b_hbm, b_ref),
-        local(6, gate_hbm, gate_w),
-        local(7, up_hbm, up_w),
-        local(8, down_hbm, down_w),
-        local(9, proj_hbm, gate_w),
+        local(0, cot_hbm.at[0, :, 0:width], column.at[here, 0]),
+        local(1, cot_hbm.at[0, :, width : 2 * width], column.at[here, 1]),
+        local(2, stream_hbm.at[0], grad_ref),
+        local(3, u_hbm.at[0], u_ref),
+        local(4, c_hbm.at[0], c_ref),
+        local(5, b_hbm.at[0], b_ref),
+        local(6, gate_hbm.at[0], gate_w),
+        local(7, up_hbm.at[0], up_w),
+        local(8, down_hbm.at[0], down_w),
+        local(9, proj_hbm.at[0], gate_w),
+        local(10, route_hbm, route_ref),
+        local(11, weight_hbm, weight_ref),
+        local(12, gain_hbm, gain_ref),
+        local(13, taps_hbm, taps_ref),
     ]
-    for copy in loads[:9]:
+    for copy in loads[10:] + loads[:9]:
         copy.start()
 
     def hop(way, block, piece):
@@ -222,7 +217,7 @@
 
     def part_copy(block, half):
         return remote(
-            part_ref.at[block, :, half * width : (half + 1) * width],
+            part_ref.at[:, half * width : (half + 1) * width],
             theirs_ref.at[block, :, half * width : (half + 1) * width],
             part_send.at[block, half],
             part_recv.at[block, half],
@@ -261,7 +256,7 @@
 
     def mixed(i):
         return remote(
-            mixed_ref,
+            near_ref.at[span(place * tokens, tokens)],
             near_ref.at[span(place * tokens, tokens)],
             mixed_send.at[i],
             mixed_recv.at[i],
@@ -317,7 +312,7 @@
     def share(part, j):
         target = part * per_part + j
         return remote(
-            share_ref.at[part, span(j * depth, depth)],
+            gate_pre_ref.at[span(part * sliver + j * depth, depth)],
             stack_ref.at[here],
             share_send.at[part, j],
             share_recv.at[here],
@@ -326,7 +321,7 @@
 
     def share_from(source):
         return remote(
-            share_ref.at[0, pl.ds(0, depth)],
+            gate_pre_ref.at[pl.ds(0, depth)],
             stack_ref.at[source],
             share_send.at[0, 0],
             share_recv.at[source],
@@ -336,21 +331,22 @@
     edge_copy = remote(edge_ref, edge_next, edge_send, edge_recv, sp=me - 1)
 
 
-    def prepare(block, way):
+    def places(block):
         wanted = lax.broadcasted_iota(jnp.int32, (bunch, tokens), 0) + here * bunch
         wanted = wanted.astype(f32)
-        first = wanted == small_ref[block, 0:1, :]
-        second = wanted == small_ref[block, 1:2, :]
+        return wanted == small_ref[block, 0:1, :], wanted == small_ref[block, 1:2, :]
+
+    def prepare(block, way):
+        first, second = places(block)
         select_ref[way] = jnp.where(first | second, 1.0, 0.0).astype(bf16)
-        weight = jnp.where(first, small_ref[block, 2:3, :], 0.0) + jnp.where(
-            second, small_ref[block, 3:4, :], 0.0
-        )
-        scale = jnp.sum(weight, axis=1, keepdims=True)
-        scale_ref[way] = jnp.broadcast_to(scale, (bunch, scale_ref.shape[2]))
 
     def pick(block, way, piece):
         chosen = jnp.dot(select_ref[way], column[block, piece], preferred_element_type=f32)
-        scale = jnp.where(piece < 2, scale_ref[way][:, 0:1], 1.0)
+
+        first, second = places(block)
+        weight = jnp.where(first, small_ref[block, 2:3, :], 0.0)
+        weight += jnp.where(second, small_ref[block, 3:4, :], 0.0)
+        scale = jnp.where(piece < 2, jnp.sum(weight, axis=1, keepdims=True), 1.0)
         outgoing[block, piece] = (chosen * scale).astype(bf16)
         kind, part = stripe(piece)
         rows_ref[kind, part, span(block * bunch + place * capacity, capacity)] = outgoing[
@@ -371,6 +367,8 @@
 
     pl.semaphore_signal(barrier, inc=1, device_id={"tp": other}, device_id_type=MESH)
     with jax.named_scope("slots"):
+        for i in range(10, 14):
+            loads[i].wait()
         names = route_ref[...].astype(f32)
         expert_row = lax.broadcasted_iota(jnp.int32, (count, tokens), 0).astype(f32)
         named = [jnp.where(expert_row == names[k : k + 1, :], 1.0, 0.0) for k in range(2)]
@@ -394,7 +392,7 @@
         loads[2].wait()
         total = jnp.zeros((tokens, lanes), f32)
         for start in range(0, 2 * width, lanes):
-            value = stream_ref[:, start : start + lanes].astype(f32)
+            value = grad_ref[:, start : start + lanes].astype(f32)
             total = total + value * value
         square_ref[...] = total
         loads[0].wait()
@@ -421,27 +419,24 @@
                 onward(way, here, piece)
         prepare(here, 0)
         for piece in range(2):
-            pick(here, 0, piece)
+            pick(here, 0, jnp.int32(piece))
         swap(0).wait_recv()
         total = square_ref[...] + square_other[...]
         inverse = lax.rsqrt(jnp.sum(total, axis=1, keepdims=True) / (4 * width) + EPSILON)
         for piece in range(2):
             cols = slice(piece * width, (piece + 1) * width)
-            value = stream_ref[:, cols].astype(f32) * inverse * gain_ref[:, cols]
+            value = grad_ref[:, cols].astype(f32) * inverse * gain_ref[:, cols]
             column[here, 2 + piece] = value.astype(bf16)
         for piece in range(2, 4):
             for way in range(2):
                 onward(way, here, piece)
         for piece in range(2, 4):
-            pick(here, 0, piece)
+            pick(here, 0, jnp.int32(piece))
         @pl.when(me == 0)
         def _():
             rim_ref[...] = jnp.zeros_like(rim_ref)
 
-        spots = jnp.transpose(small_ref[here])
-        slot = lax.broadcasted_iota(jnp.int32, pull_ref.shape, 1).astype(f32)
-        hit = (slot == spots[:, 0:1]) | (slot == spots[:, 1:2])
-        pull_ref[...] = jnp.where(hit, 1.0, 0.0).astype(bf16)
+        spots_ref[...] = jnp.transpose(small_ref[here])
 
         @pl.loop(1, planes)
         def _(i):
@@ -472,19 +467,22 @@
 
                 pick(block, way, piece)
 
+    def collect(block, piece):
+        @pl.loop(1, group)
+        def _(i):
+            inplane(block, piece, i).wait_recv()
+
+        cross(block, piece).start()
+
     def gather(step, way):
         block = here - step + 2 * way * step
         valid = (block >= 0) & (block < planes) & ((way == 0) | (step > 0))
 
         @pl.when(valid)
         def _():
-            @pl.loop(0, 4)
+            @pl.loop(0, 3)
             def _(piece):
-                @pl.loop(1, group)
-                def _(i):
-                    inplane(block, piece, i).wait_recv()
-
-                cross(block, piece).start()
+                collect(block, piece)
 
     def compute(step, way):
         block = here - step + 2 * way * step
@@ -492,20 +490,24 @@
 
         @pl.when(valid)
         def _():
-            @pl.loop(0, 4)
-            def _(piece):
-                cross(block, piece).wait_recv()
-
             rows = span(block * bunch, bunch)
             gate_lin = jnp.zeros((bunch, gate_w.shape[1]), f32)
             up_lin = jnp.zeros((bunch, gate_w.shape[1]), f32)
             hidden_grad = jnp.zeros((bunch, gate_w.shape[1]), f32)
+            for piece in range(2):
+                cross(block, piece).wait_recv()
             for part in range(4):
                 cols = slice(part * width, (part + 1) * width)
-                inputs = rows_ref[1, part, rows]
-                gate_lin += jnp.dot(inputs, gate_w[cols], preferred_element_type=f32)
-                up_lin += jnp.dot(inputs, up_w[cols], preferred_element_type=f32)
                 hidden_grad += contract_cols(rows_ref[0, part, rows], down_w[:, cols])
+            for piece in range(2, 4):
+                if piece == 3:
+                    collect(block, piece)
+                cross(block, piece).wait_recv()
+                for part in range(piece - 2, 4, 2):
+                    cols = slice(part * width, (part + 1) * width)
+                    inputs = rows_ref[1, part, rows]
+                    gate_lin += jnp.dot(inputs, gate_w[cols], preferred_element_type=f32)
+                    up_lin += jnp.dot(inputs, up_w[cols], preferred_element_type=f32)
             sigmoid_gate = jax.nn.sigmoid(gate_lin)
             silu_gate = gate_lin * sigmoid_gate
             hidden_ref[rows] = (silu_gate * up_lin).astype(bf16)
@@ -523,7 +525,7 @@
                 return value.astype(bf16)
 
             for half in range(2):
-                part_ref[block, :, half * width : (half + 1) * width] = partial(other, half)
+                part_ref[:, half * width : (half + 1) * width] = partial(other, half)
                 part_copy(block, half).start()
             for half in range(2):
                 cols = slice(half * width, (half + 1) * width)
@@ -531,25 +533,8 @@
                 part_copy(block, half).wait_recv()
                 theirs = theirs_ref[block, :, cols].astype(f32)
                 theirs_ref[block, :, cols] = (mine + theirs).astype(bf16)
-
-    def written(i):
-        mine, target = (
-            (grad_ref, grad_hbm),
-            (proj_out, proj_hbm_out),
-            (u_out, u_hbm_out),
-            (b_out, b_hbm_out),
-            (c_out, c_hbm_out),
-        )[i]
-        return pltpu.make_async_copy(mine, target, finish.at[i])
-
-    def stored(part):
-        slot = lax.rem(part, 2)
-        spot = span(part * width, width)
-        return [
-            pltpu.make_async_copy(stage_ref.at[slot, 0], gate_out.at[spot], store.at[slot, 0]),
-            pltpu.make_async_copy(stage_ref.at[slot, 1], up_out.at[spot], store.at[slot, 1]),
-            pltpu.make_async_copy(tall_ref.at[slot], down_out.at[:, spot], store.at[slot, 2]),
-        ]
+            for half in range(2):
+                part_copy(block, half).wait_send()
 
     def reply(step, way):
         block = here - step + 2 * way * step
@@ -558,7 +543,9 @@
         @pl.when(valid)
         def _():
             @pl.loop(0, group)
-            def _(i):
+            def _(turn):
+                i = lax.rem(place + turn, group)
+
                 @pl.when(block * group + i != me)
                 def _():
                     back(block, i).start()
@@ -570,62 +557,58 @@
                     ]
 
     def convolve():
-        with jax.named_scope("conv"):
-
+        gated = c_ref[...].astype(f32) * u_ref[...].astype(f32)
+        rim_gated = rim_ref[1].astype(f32) * rim_ref[0].astype(f32)
+        row = lax.broadcasted_iota(jnp.int32, gated.shape, 0)
+        one = jnp.where(row == 0, rim_gated[rim - 1 : rim], pltpu.roll(gated, 1, 0))
+        two = jnp.where(
+            row == 0,
+            rim_gated[rim - 2 : rim - 1],
+            jnp.where(row == 1, rim_gated[rim - 1 : rim], pltpu.roll(gated, 2, 0)),
+        )
+        conv = taps_ref[0:1, :] * two + taps_ref[1:2, :] * one + taps_ref[2:3, :] * gated
+        return conv
+
+    inside = (here > 0) & (here < planes - 1)
+
+    @pl.loop(1, planes + 1)
+    def _(step):
+        with jax.named_scope("arrive0"):
+
+            @pl.loop(0, 2)
+            def _(piece):
+                arrive(step, piece)
+
+        with jax.named_scope("gather"):
+
+            @pl.loop(0, 2)
+            def _(way):
+                gather(step - 1, way)
+
+        @pl.loop(0, 2)
+        def _(way):
+            with jax.named_scope("compute"):
+                compute(step - 1, way)
+
+        with jax.named_scope("arrive2"):
+
+            @pl.loop(2, 4)
+            def _(piece):
+                arrive(step, piece)
+
+        @pl.loop(0, 2)
+        def _(way):
+            reply(step - 1, way)
+
+        @pl.when(step == 1)
+        def _():
             @pl.when(me > 0)
             def _():
                 for i in range(2):
                     rim_copy(i).wait_recv()
 
-            gated = c_ref[...].astype(f32) * u_ref[...].astype(f32)
-            rim_gated = rim_ref[1].astype(f32) * rim_ref[0].astype(f32)
-            row = lax.broadcasted_iota(jnp.int32, gated.shape, 0)
-            one = jnp.where(row == 0, rim_gated[rim - 1 : rim], pltpu.roll(gated, 1, 0))
-            two = jnp.where(
-                row == 0,
-                rim_gated[rim - 2 : rim - 1],
-                jnp.where(row == 1, rim_gated[rim - 1 : rim], pltpu.roll(gated, 2, 0)),
-            )
-            conv = taps_ref[0:1, :] * two + taps_ref[1:2, :] * one + taps_ref[2:3, :] * gated
-            conv_ref[...] = conv
-            mixed_value = (b_ref[...].astype(f32) * conv).astype(bf16)
-            mixed_ref[...] = mixed_value
-            near_ref[span(place * tokens, tokens)] = mixed_value
-
-    inside = (here > 0) & (here < planes - 1)
-
-    @pl.loop(1, planes + 1)
-    def _(step):
-        with jax.named_scope("arrive0"):
-
-            @pl.loop(0, 2)
-            def _(piece):
-                arrive(step, piece)
-
-        with jax.named_scope("gather"):
-
-            @pl.loop(0, 2)
-            def _(way):
-                gather(step - 1, way)
-
-        @pl.loop(0, 2)
-        def _(way):
-            with jax.named_scope("compute"):
-                compute(step - 1, way)
-
-        with jax.named_scope("arrive2"):
-
-            @pl.loop(2, 4)
-            def _(piece):
-                arrive(step, piece)
-
-        @pl.loop(0, 2)
-        def _(way):
-            reply(step - 1, way)
-
-        @pl.when(step == 1)
-        def _():
-            convolve()
+            mixed_value = b_ref[...].astype(f32) * convolve()
+            near_ref[span(place * tokens, tokens)] = mixed_value.astype(bf16)
 
         @pl.when(step == jnp.where(inside, planes, 2))
         def _():
@@ -636,21 +619,40 @@
     loads[9].start()
     with jax.named_scope("wgrad"):
 
+        for part in range(4):
+            inputs = rows_ref[1, part]
+            pieces[part][...] = contract_rows(inputs, gate_pre_ref[...])
+            pieces[4 + part][...] = contract_rows(inputs, up_pre_ref[...])
+            pieces[8 + part][...] = contract_rows(hidden_ref[...], rows_ref[0, part])
+
+    @pl.loop(0, planes)
+    def _(block):
         @pl.loop(0, 4)
-        def _(part):
-            slot = lax.rem(part, 2)
-
-            @pl.when(part >= 2)
-            def _():
-                for copy in stored(part - 2):
-                    copy.wait()
-
-            inputs = rows_ref[1, part]
-            stage_ref[slot, 0] = contract_rows(inputs, gate_pre_ref[...])
-            stage_ref[slot, 1] = contract_rows(inputs, up_pre_ref[...])
-            tall_ref[slot] = contract_rows(hidden_ref[...], rows_ref[0, part])
-            for copy in stored(part):
-                copy.start()
+        def _(piece):
+            for way in range(2):
+                room = here < planes - 1 if way == 0 else here > 0
+                mine = block <= here if way == 0 else block >= here
+
+                @pl.when(room & mine)
+                def _():
+                    hop(way, block, piece).wait_send()
+
+            cross(block, piece).wait_send()
+
+            @pl.loop(1, group)
+            def _(i):
+                inplane(block, piece, i).wait_send()
+
+    @pl.loop(1, planes)
+    def _(i):
+        small(i).wait_send()
+
+    @pl.when(me < count - 1)
+    def _():
+        for i in range(2):
+            rim_copy(i).wait_send()
+
+    swap(0).wait_send()
 
     @pl.loop(0, planes)
     def _(turn):
@@ -665,7 +667,11 @@
 
         with jax.named_scope("pull"):
             rows = span(block * bunch, bunch)
-            value = jnp.dot(pull_ref[:, rows], ret_ref[rows], preferred_element_type=f32)
+            slot = lax.broadcasted_iota(jnp.int32, (tokens, bunch), 1) + block * bunch
+            slot = slot.astype(f32)
+            hit = (slot == spots_ref[:, 0:1]) | (slot == spots_ref[:, 1:2])
+            pull = jnp.where(hit, 1.0, 0.0).astype(bf16)
+            value = jnp.dot(pull, ret_ref[rows], preferred_element_type=f32)
 
             @pl.when(turn == 0)
             def _():
@@ -679,7 +685,7 @@
         total = jnp.zeros((tokens, lanes), f32)
         for start in range(0, 2 * width, lanes):
             cols = slice(start, start + lanes)
-            total += stream_ref[:, cols].astype(f32) * gain_ref[:, cols] * total_ref[:, cols]
+            total += grad_ref[:, cols].astype(f32) * gain_ref[:, cols] * total_ref[:, cols]
         inner_ref[...] = total
         swap(1).start()
         square = jnp.sum(square_ref[...] + square_other[...], axis=1, keepdims=True)
@@ -692,10 +698,9 @@
             grad_ref[:, cols] = (
                 column[here, piece].astype(f32)
                 + inverse * gain_ref[:, cols] * total_ref[:, cols]
-                - stream_ref[:, cols].astype(f32) * pull_back
+                - grad_ref[:, cols].astype(f32) * pull_back
             ).astype(bf16)
         swap(2).start()
-        written(0).start()
 
     upper = here >= planes // 2
     base = lax.div(here * parts, planes)
@@ -752,8 +757,7 @@
         def _():
             edge_copy.start()
 
-        b_out[...] = (mixer_grad * conv_ref[...]).astype(bf16)
-        written(3).start()
+        b_out[...] = (mixer_grad * convolve()).astype(bf16)
 
     @pl.loop(1, group)
     def _(i):
@@ -780,7 +784,7 @@
 
         with jax.named_scope("shares"):
             value = contract_rows(block_ref[part], near_ref[...])
-            share_ref[part] = value.astype(bf16)
+            gate_pre_ref[span(part * sliver, sliver)] = value.astype(bf16)
             for j in range(per_part):
 
                 @pl.when(part * per_part + j != here)
@@ -813,12 +817,33 @@
         gated_grad = taps_ref[2:3, :] * delta + taps_ref[1:2, :] * one + taps_ref[0:1, :] * two
         u_out[...] = (gated_grad * c_ref[...].astype(f32)).astype(bf16)
         c_out[...] = (gated_grad * u_ref[...].astype(f32)).astype(bf16)
-        written(2).start()
-        written(4).start()
-
-    for part in range(2, 4):
-        for copy in stored(part):
-            copy.wait()
+
+    @pl.loop(0, planes)
+    def _(block):
+        @pl.loop(0, group)
+        def _(i):
+            @pl.when(block * group + i != me)
+            def _():
+                back(block, i).wait_send()
+
+    @pl.when(me > 0)
+    def _():
+        edge_copy.wait_send()
+
+    for i in range(1, 3):
+        swap(i).wait_send()
+
+    @pl.loop(0, parts)
+    def _(part):
+        @pl.when(owned(part))
+        def _():
+            @pl.loop(0, group)
+            def _(target):
+                @pl.when(target != place)
+                def _():
+                    spread(target, part).wait_send()
+
+            hand(part).wait_send()
 
     with jax.named_scope("final"):
 
@@ -828,71 +853,38 @@
             share_from(source).wait_recv()
             proj_out[...] += stack_ref[source].astype(f32)
 
-    written(1).start()
-
-    @pl.loop(0, planes)
-    def _(block):
-        @pl.loop(0, 4)
-        def _(piece):
-            for way in range(2):
-                room = here < planes - 1 if way == 0 else here > 0
-                mine = block <= here if way == 0 else block >= here
-
-                @pl.when(room & mine)
-                def _():
-                    hop(way, block, piece).wait_send()
-
-            cross(block, piece).wait_send()
-
-            @pl.loop(1, group)
-            def _(i):
-                inplane(block, piece, i).wait_send()
-
-        for half in range(2):
-            part_copy(block, half).wait_send()
-
-        @pl.loop(0, group)
-        def _(i):
-            @pl.when(block * group + i != me)
-            def _():
-                back(block, i).wait_send()
-
-    @pl.loop(1, planes)
-    def _(i):
-        small(i).wait_send()
-
-    @pl.when(me < count - 1)
-    def _():
-        for i in range(2):
-            rim_copy(i).wait_send()
-
-    @pl.when(me > 0)
-    def _():
-        edge_copy.wait_send()
-
-    for i in range(3):
-        swap(i).wait_send()
-
     @pl.loop(0, parts)
     def _(part):
-        @pl.when(owned(part))
-        def _():
-            @pl.loop(0, group)
-            def _(target):
-                @pl.when(target != place)
-                def _():
-                    spread(target, part).wait_send()
-
-            hand(part).wait_send()
-
         for j in range(per_part):
 
             @pl.when(part * per_part + j != here)
             def _():
                 share(part, j).wait_send()
 
-    for i in range(5):
-        written(i).wait()
+
+def store_kernel(*refs):
+    sources, targets, sems = refs[:17], refs[17:25], refs[25]
+    copies = []
+    for i in range(17):
+        if i < 5:
+            target = targets[i]
+        else:
+            which, part = (i - 5) // 4, (i - 5) % 4
+            rows, cols = sources[i].shape
+            target = targets[5 + which]
+            if which < 2:
+                target = target.at[pl.ds(part * rows, rows)]
+            else:
+                target = target.at[:, pl.ds(part * cols, cols)]
+        copies.append(pltpu.make_async_copy(sources[i], target, sems.at[i]))
+    for copy in copies:
+        copy.start()
+    for copy in copies:
+        copy.wait()
+
+
+def pinned(value):
+    return pltpu.with_memory_space_constraint(value, pltpu.HBM)
 
 
 def local(
@@ -921,6 +913,7 @@
     capacity = 2 * tokens * routes.shape[1] // count
     bunch = group * capacity
     slots = count * capacity
+    grant = 38 * MIB + 2 * planes * tokens * features * 2
     depth = 2 * features // count
     sliver = max(128, depth)
     parts = planes * depth // sliver
@@ -940,10 +933,16 @@
     dma = pltpu.SemaphoreType.DMA
     results = pl.pallas_call(
         lambda *refs: layer_kernel(planes, group, *refs),
-        out_shape=outs,
-        in_specs=[hbm, vmem, hbm, vmem, vmem, hbm, hbm, hbm, vmem, hbm, hbm, hbm, hbm],
-        out_specs=[hbm] * 8,
+        out_shape=tuple(pltpu.VMEM(out.shape, out.dtype) for out in outs[:5])
+        + (pltpu.VMEM((width, hidden), f32),) * 8
+        + (pltpu.VMEM((hidden, width), f32),) * 4,
+        in_specs=[hbm] * 13,
+        out_specs=[vmem] * 17,
         scratch_shapes=[
+            pltpu.VMEM((1, features), f32),
+            pltpu.VMEM(route_weights.shape[::-1], f32),
+            pltpu.VMEM(routes.shape[::-1], jnp.int32),
+            pltpu.VMEM(conv_taps.shape, f32),
             pltpu.VMEM((planes, 4, tokens, width), bf16),
             pltpu.VMEM((planes, 4, bunch, width), bf16),
             pltpu.VMEM((2, 4, slots, width), bf16),
@@ -953,43 +952,29 @@
             pltpu.VMEM((slots, hidden), bf16),
             pltpu.VMEM((slots, hidden), bf16),
             pltpu.VMEM((slots, hidden), bf16),
-            pltpu.VMEM((planes, bunch, features), bf16),
+            pltpu.VMEM((bunch, features), bf16),
             pltpu.VMEM((planes, bunch, features), bf16),
             pltpu.VMEM((slots, features), bf16),
-            pltpu.VMEM((tokens, features), bf16),
             pltpu.VMEM((tokens, channels), bf16),
             pltpu.VMEM((tokens, channels), bf16),
             pltpu.VMEM((tokens, channels), bf16),
-            pltpu.VMEM((tokens, channels), f32),
             pltpu.VMEM((group * tokens, channels), bf16),
             pltpu.VMEM((2, 16, channels), bf16),
-            pltpu.VMEM((tokens, channels), bf16),
             pltpu.VMEM((planes, 8, tokens), f32),
             pltpu.VMEM((tokens, 128), f32),
             pltpu.VMEM((tokens, 128), f32),
             pltpu.VMEM((tokens, 128), f32),
             pltpu.VMEM((tokens, 128), f32),
             pltpu.VMEM((2, bunch, tokens), bf16),
-            pltpu.VMEM((2, bunch, 128), f32),
-            pltpu.VMEM((tokens, slots), bf16),
+            pltpu.VMEM((tokens, 8), f32),
             pltpu.VMEM((tokens, features), f32),
             pltpu.VMEM((tokens, features), bf16),
             pltpu.VMEM((parts, group * tokens, sliver), bf16),
-            pltpu.VMEM((parts, sliver, channels), bf16),
             pltpu.VMEM((planes, depth, channels), bf16),
             pltpu.VMEM((8, channels), f32),
             pltpu.VMEM((8, channels), f32),
-            pltpu.VMEM(stream.shape, bf16),
-            pltpu.VMEM((depth, channels), f32),
-            pltpu.VMEM(conv_input.shape, bf16),
-            pltpu.VMEM(conv_input.shape, bf16),
-            pltpu.VMEM(conv_input.shape, bf16),
             pltpu.VMEM(stream.shape if sliver > depth else (8, 128), bf16),
-            pltpu.VMEM((2, 2, width, hidden), f32),
-            pltpu.VMEM((2, hidden, width), f32),
-            dma((10,)),
-            dma((2, 3)),
-            dma((5,)),
+            dma((14,)),
             dma((2, planes, 4)),
             dma((planes, 4)),
             dma((planes, 4, group)),
@@ -1018,25 +1003,34 @@
             dma,
         ],
         compiler_params=pltpu.CompilerParams(
-            collective_id=0, has_side_effects=True, vmem_limit_bytes=VMEM_LIMIT
+            collective_id=0, has_side_effects=True, vmem_limit_bytes=grant
         ),
         name="layer",
     )(
-        stream,
-        norm_gain[None, :],
-        cotangent,
-        route_weights.T,
-        routes.T,
-        conv_input,
-        conv_bgate,
-        conv_cgate,
-        conv_taps,
-        out_proj,
-        gate_weight[0],
-        up_weight[0],
-        down_weight[0],
+        pinned(stream[None]),
+        pinned(norm_gain[None, :]),
+        pinned(cotangent[None]),
+        pinned(route_weights.T),
+        pinned(routes.T),
+        pinned(conv_input[None]),
+        pinned(conv_bgate[None]),
+        pinned(conv_cgate[None]),
+        pinned(conv_taps),
+        pinned(out_proj[None]),
+        pinned(gate_weight),
+        pinned(up_weight),
+        pinned(down_weight),
     )
-    return results[:5] + tuple(value[None] for value in results[5:])
+    results = pl.pallas_call(
+        store_kernel,
+        out_shape=outs,
+        in_specs=[vmem] * 17,
+        out_specs=[hbm] * 8,
+        scratch_shapes=[dma((17,))],
+        compiler_params=pltpu.CompilerParams(vmem_limit_bytes=2**20),
+        name="store",
+    )(*results)
+    return tuple(results[:5]) + tuple(value[None] for value in results[5:])
 
 
 def solution(mesh):

time: 158 us -> 138 us (0.87)
  local copies, waits for them, and re-layouts: 19.1 us -> 0 us
    unnamed x12 -> x0, local copies, waits for them, and re-layouts: 19.1 us -> none
    pallas_call x1, Pallas kernels: 137 us -> 132 us  [local(): pl.pallas_call(lambda *refs: layer_kernel(planes, group, *refs), out_shap...]
    pallas_call x0 -> x1, Pallas kernels: none -> 5.21 us  [local(): pl.pallas_call(store_kernel, out_shape=outs, in_specs=[vmem] * 17, out_sp...]
where the time goes in v3:
time: 138 us
  Pallas kernels  137 us (99%)
    pallas_call x1, Pallas kernels, local(): pl.pallas_call(lambda *refs: layer_kernel(planes, group, *refs), out_shap...  132 us
    pallas_call x1, Pallas kernels, local(): pl.pallas_call(store_kernel, out_shape=outs, in_specs=[vmem] * 17, out_sp...  5.21 us

profile of v3, /device:TPU:17, one launch (start us, length us, event | category | flops | bytes accessed | tf_op | source)
XLA Modules:
  0.0 137.7 jit_solution(6998766948309186111)
XLA Ops:
  0.6 131.8 %layer.1 = (bf16[256,1024]{1,0:T(8,128)(2,1)S(1)}, f32[128,512]{1,0:T(8,128)S(1)}, bf16[256,512]{1,0:T(8,128)(2,1)S(1)}, bf16[256,512]{1,0:T(8,128)(2,1)S(1)}, b...) custom-call(bf16[1,256,1024]{2,1,0:T(8,128)(2,1)} %bitcast.13, ...), custom_call_target="tpu_custom_call" | custom-call | tf_op jit(solution)/shard_map/layer/pallas_call | solution.py:934
  132.5 5.2 %store.1 = (bf16[256,1024]{1,0:T(8,128)(2,1)}, f32[128,512]{1,0:T(8,128)}, bf16[256,512]{1,0:T(8,128)(2,1)}, bf16[256,512]{1,0:T(8,128)(2,1)}, bf16[256,512]{1,0...) custom-call(bf16[256,1024]{1,0:T(8,128)(2,1)S(1)} %get-tuple-element.33.refs_0_, ...), custom_call_target="tpu_custom_call" | custom-call | tf_op jit(solution)/shard_map/store/pallas_call | solution.py:1024

commit v4 on v3

--- a/solution.py
+++ b/solution.py
@@ -161,7 +161,7 @@
         return remote(
             spot,
             spot,
-            hop_send.at[way, block, piece],
+            hop_send.at[way, block],
             hop_recv.at[block, piece],
             sp=me + (1 - 2 * way) * group,
         )
@@ -177,19 +177,13 @@
         return remote(
             small_ref.at[here],
             small_ref.at[here],
-            small_send.at[i],
-            small_recv.at[i],
+            small_send,
+            small_recv,
             sp=lax.rem(here + i, planes) * group + place,
         )
 
-    def small_from(i):
-        return remote(
-            small_ref.at[here],
-            small_ref.at[lax.rem(here + planes - i, planes)],
-            small_send.at[i],
-            small_recv.at[i],
-            sp=lax.rem(here + i, planes) * group + place,
-        )
+    def every(spot, sent, received):
+        return remote(spot, spot, sent, received, tp=other)
 
     def stripe(piece):
         return lax.div(piece, 2), 2 * side + lax.rem(piece, 2)
@@ -203,8 +197,8 @@
         return remote(
             outgoing.at[block, piece, span(target * capacity, capacity)],
             rows_ref.at[kind, part, span(block * bunch + place * capacity, capacity)],
-            plane_send.at[block, piece, i],
-            plane_recv.at[block, piece, i],
+            plane_send.at[block],
+            plane_recv.at[block, piece],
             sp=here * group + target,
         )
 
@@ -212,14 +206,14 @@
         kind, part = stripe(piece)
         spot = rows_ref.at[kind, part, span(block * bunch, bunch)]
         return remote(
-            spot, spot, cross_send.at[block, piece], cross_recv.at[block, piece], tp=other
+            spot, spot, cross_send.at[block], cross_recv.at[block, piece], tp=other
         )
 
     def part_copy(block, half):
         return remote(
             part_ref.at[:, half * width : (half + 1) * width],
             theirs_ref.at[block, :, half * width : (half + 1) * width],
-            part_send.at[block, half],
+            part_send.at[half],
             part_recv.at[block, half],
             tp=other,
         )
@@ -228,19 +222,24 @@
         return remote(
             theirs_ref.at[block, span(i * capacity, capacity)],
             ret_ref.at[span(me * capacity, capacity)],
-            back_send.at[block, i],
-            back_recv.at[me],
+            back_send.at[block],
+            back_recv.at[here],
             sp=block * group + i,
         )
 
-    def back_from(source):
-        return remote(
-            theirs_ref.at[0, pl.ds(0, capacity)],
-            ret_ref.at[span(source * capacity, capacity)],
-            back_send.at[0, 0],
-            back_recv.at[source],
-            sp=source,
-        )
+    def backs(block, rows):
+        return every(
+            ret_ref.at[pl.ds(0, rows * capacity)], back_send.at[block], back_recv.at[block]
+        )
+
+    def for_backs(block, act):
+        @pl.when(block == here)
+        def _():
+            act(backs(block, group - 1))
+
+        @pl.when(block != here)
+        def _():
+            act(backs(block, group))
 
     rim = rim_ref.shape[1]
 
@@ -249,17 +248,20 @@
         return remote(
             source.at[tokens - rim : tokens],
             rim_ref.at[i],
-            rim_send.at[i],
-            rim_recv.at[i],
+            rim_send,
+            rim_recv,
             sp=me + 1,
         )
+
+    rims = every(rim_ref, rim_send, rim_recv)
+    mixes = every(near_ref.at[pl.ds(0, (group - 1) * tokens)], mixed_send, mixed_recv)
 
     def mixed(i):
         return remote(
             near_ref.at[span(place * tokens, tokens)],
             near_ref.at[span(place * tokens, tokens)],
-            mixed_send.at[i],
-            mixed_recv.at[i],
+            mixed_send,
+            mixed_recv,
             sp=here * group + lax.rem(place + i, group),
         )
 
@@ -291,19 +293,14 @@
         return remote(
             strip(target, part),
             block_ref.at[part, span(place * tokens, tokens)],
-            spread_send.at[target, part],
-            spread_recv.at[place, part],
+            spread_send.at[part],
+            spread_recv.at[part],
             sp=here * group + target,
         )
 
-    def spread_from(source, part):
-        return remote(
-            grad_ref.at[:, pl.ds(0, sliver)],
-            block_ref.at[part, span(source * tokens, tokens)],
-            spread_send.at[source, part],
-            spread_recv.at[source, part],
-            sp=here * group + source,
-        )
+    def spreads(part):
+        spot = block_ref.at[part, pl.ds(0, (group - 1) * tokens)]
+        return every(spot, spread_send.at[part], spread_recv.at[part])
 
     def hand(part):
         spot = block_ref.at[part]
@@ -314,7 +311,7 @@
         return remote(
             gate_pre_ref.at[span(part * sliver + j * depth, depth)],
             stack_ref.at[here],
-            share_send.at[part, j],
+            share_send,
             share_recv.at[here],
             sp=target * group + place,
         )
@@ -323,7 +320,7 @@
         return remote(
             gate_pre_ref.at[pl.ds(0, depth)],
             stack_ref.at[source],
-            share_send.at[0, 0],
+            share_send,
             share_recv.at[source],
             sp=source * group + place,
         )
@@ -438,9 +435,8 @@
 
         spots_ref[...] = jnp.transpose(small_ref[here])
 
-        @pl.loop(1, planes)
-        def _(i):
-            small_from(i).wait_recv()
+        smalls = every(small_ref.at[pl.ds(0, planes - 1)], small_send, small_recv)
+        smalls.wait_recv()
 
         for i in range(5, 9):
             loads[i].wait()
@@ -468,10 +464,8 @@
                 pick(block, way, piece)
 
     def collect(block, piece):
-        @pl.loop(1, group)
-        def _(i):
-            inplane(block, piece, i).wait_recv()
-
+        spot = outgoing.at[block, piece, pl.ds(0, (group - 1) * capacity)]
+        every(spot, plane_send.at[block], plane_recv.at[block, piece]).wait_recv()
         cross(block, piece).start()
 
     def gather(step, way):
@@ -604,8 +598,7 @@
         def _():
             @pl.when(me > 0)
             def _():
-                for i in range(2):
-                    rim_copy(i).wait_recv()
+                rims.wait_recv()
 
             mixed_value = b_ref[...].astype(f32) * convolve()
             near_ref[span(place * tokens, tokens)] = mixed_value.astype(bf16)
@@ -627,30 +620,23 @@
 
     @pl.loop(0, planes)
     def _(block):
-        @pl.loop(0, 4)
-        def _(piece):
-            for way in range(2):
-                room = here < planes - 1 if way == 0 else here > 0
-                mine = block <= here if way == 0 else block >= here
-
-                @pl.when(room & mine)
-                def _():
-                    hop(way, block, piece).wait_send()
-
-            cross(block, piece).wait_send()
-
-            @pl.loop(1, group)
-            def _(i):
-                inplane(block, piece, i).wait_send()
-
-    @pl.loop(1, planes)
-    def _(i):
-        small(i).wait_send()
+        for way in range(2):
+            room = here < planes - 1 if way == 0 else here > 0
+            mine = block <= here if way == 0 else block >= here
+
+            @pl.when(room & mine)
+            def _():
+                every(column.at[block], hop_send.at[way, block], hop_recv.at[0, 0]).wait_send()
+
+        every(outgoing.at[block], cross_send.at[block], cross_recv.at[0, 0]).wait_send()
+        spot = outgoing.at[block, :, pl.ds(0, (group - 1) * capacity)]
+        every(spot, plane_send.at[block], plane_recv.at[0, 0]).wait_send()
+
+    smalls.wait_send()
 
     @pl.when(me < count - 1)
     def _():
-        for i in range(2):
-            rim_copy(i).wait_send()
+        rims.wait_send()
 
     swap(0).wait_send()
 
@@ -659,11 +645,7 @@
         block = lax.rem(here + turn, planes)
         with jax.named_scope("returned"):
 
-            @pl.loop(0, group)
-            def _(i):
-                @pl.when(block * group + i != me)
-                def _():
-                    back_from(block * group + i).wait_recv()
+            for_backs(block, lambda copy: copy.wait_recv())
 
         with jax.named_scope("pull"):
             rows = span(block * bunch, bunch)
@@ -726,19 +708,26 @@
                     preferred_element_type=f32,
                 ).astype(bf16)
 
-        @pl.loop(0, parts)
-        def _(k):
-            part = turned(k)
-
-            @pl.when(owned(part))
-            def _():
-                @pl.loop(0, group)
-                def _(target):
-                    @pl.when(target != place)
-                    def _():
-                        spread(target, part).start()
-
-                block_ref[part, span(place * tokens, tokens)] = strip(place, part)[...]
+        def spread_all():
+            @pl.loop(0, parts)
+            def _(k):
+                part = turned(k)
+
+                @pl.when(owned(part))
+                def _():
+                    @pl.loop(0, group)
+                    def _(target):
+                        @pl.when(target != place)
+                        def _():
+                            spread(target, part).start()
+
+                    block_ref[part, span(place * tokens, tokens)] = strip(place, part)[...]
+
+        first = owned(turned(0))
+
+        @pl.when(first)
+        def _():
+            spread_all()
 
     with jax.named_scope("mixer"):
         half = 2 * width
@@ -759,9 +748,11 @@
 
         b_out[...] = (mixer_grad * convolve()).astype(bf16)
 
-    @pl.loop(1, group)
-    def _(i):
-        mixed(i).wait()
+    @pl.when(jnp.logical_not(first))
+    def _():
+        spread_all()
+
+    mixes.wait()
 
     @pl.loop(0, parts)
     def _(k):
@@ -770,12 +761,7 @@
 
             @pl.when(owned(part))
             def _():
-                @pl.loop(0, group)
-                def _(source):
-                    @pl.when(source != place)
-                    def _():
-                        spread_from(source, part).wait_recv()
-
+                spreads(part).wait_recv()
                 hand(part).start()
 
             @pl.when(jnp.logical_not(owned(part)))
@@ -820,11 +806,7 @@
 
     @pl.loop(0, planes)
     def _(block):
-        @pl.loop(0, group)
-        def _(i):
-            @pl.when(block * group + i != me)
-            def _():
-                back(block, i).wait_send()
+        for_backs(block, lambda copy: copy.wait_send())
 
     @pl.when(me > 0)
     def _():
@@ -837,12 +819,7 @@
     def _(part):
         @pl.when(owned(part))
         def _():
-            @pl.loop(0, group)
-            def _(target):
-                @pl.when(target != place)
-                def _():
-                    spread(target, part).wait_send()
-
+            spreads(part).wait_send()
             hand(part).wait_send()
 
     with jax.named_scope("final"):
@@ -853,13 +830,7 @@
             share_from(source).wait_recv()
             proj_out[...] += stack_ref[source].astype(f32)
 
-    @pl.loop(0, parts)
-    def _(part):
-        for j in range(per_part):
-
-            @pl.when(part * per_part + j != here)
-            def _():
-                share(part, j).wait_send()
+    every(stack_ref.at[pl.ds(0, planes - 1)], share_send, share_recv.at[0]).wait_send()
 
 
 def store_kernel(*refs):
@@ -975,29 +946,29 @@
             pltpu.VMEM((8, channels), f32),
             pltpu.VMEM(stream.shape if sliver > depth else (8, 128), bf16),
             dma((14,)),
-            dma((2, planes, 4)),
+            dma((2, planes)),
             dma((planes, 4)),
-            dma((planes, 4, group)),
-            dma((planes, 4, group)),
+            dma((planes,)),
             dma((planes, 4)),
+            dma((planes,)),
             dma((planes, 4)),
+            dma((2,)),
             dma((planes, 2)),
-            dma((planes, 2)),
-            dma((planes, group)),
-            dma((count,)),
             dma((planes,)),
             dma((planes,)),
-            dma((2,)),
-            dma((2,)),
+            dma,
+            dma,
+            dma,
+            dma,
             dma((3,)),
             dma((3,)),
-            dma((group,)),
-            dma((group,)),
-            dma((group, parts)),
-            dma((group, parts)),
+            dma,
+            dma,
             dma((parts,)),
             dma((parts,)),
-            dma((parts, planes // parts)),
+            dma((parts,)),
+            dma((parts,)),
+            dma,
             dma((planes,)),
             dma,
             dma,

time: 138 us -> 135 us (0.978)
  Pallas kernels: 137 us -> 134 us
    pallas_call x1, Pallas kernels: 132 us -> 129 us  [local(): pl.pallas_call(lambda *refs: layer_kernel(planes, group, *refs), out_shap...]
where the time goes in v4:
time: 135 us
  Pallas kernels  134 us (99%)
    pallas_call x1, Pallas kernels, local(): pl.pallas_call(lambda *refs: layer_kernel(planes, group, *refs), out_shap...  129 us
    pallas_call x1, Pallas kernels, local(): pl.pallas_call(store_kernel, out_shape=outs, in_specs=[vmem] * 17, out_sp...  5.21 us

profile of v4, /device:TPU:17, one launch (start us, length us, event | category | flops | bytes accessed | tf_op | source)
XLA Modules:
  0.0 134.8 jit_solution(8111840513998050928)
XLA Ops:
  0.6 128.9 %layer.1 = (bf16[256,1024]{1,0:T(8,128)(2,1)S(1)}, f32[128,512]{1,0:T(8,128)S(1)}, bf16[256,512]{1,0:T(8,128)(2,1)S(1)}, bf16[256,512]{1,0:T(8,128)(2,1)S(1)}, b...) custom-call(bf16[1,256,1024]{2,1,0:T(8,128)(2,1)} %bitcast.13, ...), custom_call_target="tpu_custom_call" | custom-call | tf_op jit(solution)/shard_map/layer/pallas_call | solution.py:905
  129.6 5.2 %store.1 = (bf16[256,1024]{1,0:T(8,128)(2,1)}, f32[128,512]{1,0:T(8,128)}, bf16[256,512]{1,0:T(8,128)(2,1)}, bf16[256,512]{1,0:T(8,128)(2,1)}, bf16[256,512]{1,0...) custom-call(bf16[256,1024]{1,0:T(8,128)(2,1)S(1)} %get-tuple-element.33.refs_0_, ...), custom_call_target="tpu_custom_call" | custom-call | tf_op jit(solution)/shard_map/store/pallas_call | solution.py:995

commit v5 on v4

--- a/solution.py
+++ b/solution.py
@@ -197,7 +197,7 @@
         return remote(
             outgoing.at[block, piece, span(target * capacity, capacity)],
             rows_ref.at[kind, part, span(block * bunch + place * capacity, capacity)],
-            plane_send.at[block],
+            plane_send,
             plane_recv.at[block, piece],
             sp=here * group + target,
         )
@@ -206,7 +206,7 @@
         kind, part = stripe(piece)
         spot = rows_ref.at[kind, part, span(block * bunch, bunch)]
         return remote(
-            spot, spot, cross_send.at[block], cross_recv.at[block, piece], tp=other
+            spot, spot, cross_send, cross_recv.at[block, piece], tp=other
         )
 
     def part_copy(block, half):
@@ -222,14 +222,14 @@
         return remote(
             theirs_ref.at[block, span(i * capacity, capacity)],
             ret_ref.at[span(me * capacity, capacity)],
-            back_send.at[block],
+            back_send,
             back_recv.at[here],
             sp=block * group + i,
         )
 
     def backs(block, rows):
         return every(
-            ret_ref.at[pl.ds(0, rows * capacity)], back_send.at[block], back_recv.at[block]
+            ret_ref.at[pl.ds(0, rows * capacity)], back_send, back_recv.at[block]
         )
 
     def for_backs(block, act):
@@ -397,6 +397,8 @@
     with jax.named_scope("greet"):
         pl.semaphore_wait(barrier, count)
     with jax.named_scope("own"):
+        for way in range(2):
+            onward(way, here, 0)
         swap(0).start()
 
         @pl.loop(1, planes)
@@ -411,9 +413,8 @@
             for i in range(2):
                 rim_copy(i).start()
 
-        for piece in range(2):
-            for way in range(2):
-                onward(way, here, piece)
+        for way in range(2):
+            onward(way, here, 1)
         prepare(here, 0)
         for piece in range(2):
             pick(here, 0, jnp.int32(piece))
@@ -465,7 +466,7 @@
 
     def collect(block, piece):
         spot = outgoing.at[block, piece, pl.ds(0, (group - 1) * capacity)]
-        every(spot, plane_send.at[block], plane_recv.at[block, piece]).wait_recv()
+        every(spot, plane_send, plane_recv.at[block, piece]).wait_recv()
         cross(block, piece).start()
 
     def gather(step, way):
@@ -628,10 +629,9 @@
             def _():
                 every(column.at[block], hop_send.at[way, block], hop_recv.at[0, 0]).wait_send()
 
-        every(outgoing.at[block], cross_send.at[block], cross_recv.at[0, 0]).wait_send()
-        spot = outgoing.at[block, :, pl.ds(0, (group - 1) * capacity)]
-        every(spot, plane_send.at[block], plane_recv.at[0, 0]).wait_send()
-
+    every(outgoing, cross_send, cross_recv.at[0, 0]).wait_send()
+    spot = outgoing.at[:, :, pl.ds(0, (group - 1) * capacity)]
+    every(spot, plane_send, plane_recv.at[0, 0]).wait_send()
     smalls.wait_send()
 
     @pl.when(me < count - 1)
@@ -804,9 +804,8 @@
         u_out[...] = (gated_grad * c_ref[...].astype(f32)).astype(bf16)
         c_out[...] = (gated_grad * u_ref[...].astype(f32)).astype(bf16)
 
-    @pl.loop(0, planes)
-    def _(block):
-        for_backs(block, lambda copy: copy.wait_send())
+    spot = ret_ref.at[pl.ds(0, (count - 1) * capacity)]
+    every(spot, back_send, back_recv.at[0]).wait_send()
 
     @pl.when(me > 0)
     def _():
@@ -948,13 +947,13 @@
             dma((14,)),
             dma((2, planes)),
             dma((planes, 4)),
-            dma((planes,)),
+            dma,
             dma((planes, 4)),
-            dma((planes,)),
+            dma,
             dma((planes, 4)),
             dma((2,)),
             dma((planes, 2)),
-            dma((planes,)),
+            dma,
             dma((planes,)),
             dma,
             dma,

time: 135 us -> 136 us (level)
  no operation moved by 1% of the time
where the time goes in v5:
time: 136 us; the launch traced here: 135 us
  Pallas kernels  134 us (99%)
    pallas_call x1, Pallas kernels, local(): pl.pallas_call(lambda *refs: layer_kernel(planes, group, *refs), out_shap...  129 us
    pallas_call x1, Pallas kernels, local(): pl.pallas_call(store_kernel, out_shape=outs, in_specs=[vmem] * 17, out_sp...  5.21 us

profile of v5, /device:TPU:17, one launch (start us, length us, event | category | flops | bytes accessed | tf_op | source)
XLA Modules:
  0.0 134.6 jit_solution(1464597636690853585)
XLA Ops:
  0.6 128.7 %layer.1 = (bf16[256,1024]{1,0:T(8,128)(2,1)S(1)}, f32[128,512]{1,0:T(8,128)S(1)}, bf16[256,512]{1,0:T(8,128)(2,1)S(1)}, bf16[256,512]{1,0:T(8,128)(2,1)S(1)}, b...) custom-call(bf16[1,256,1024]{2,1,0:T(8,128)(2,1)} %bitcast.13, ...), custom_call_target="tpu_custom_call" | custom-call | tf_op jit(solution)/shard_map/layer/pallas_call | solution.py:904
  129.4 5.2 %store.1 = (bf16[256,1024]{1,0:T(8,128)(2,1)}, f32[128,512]{1,0:T(8,128)}, bf16[256,512]{1,0:T(8,128)(2,1)}, bf16[256,512]{1,0:T(8,128)(2,1)}, bf16[256,512]{1,0...) custom-call(bf16[256,1024]{1,0:T(8,128)(2,1)S(1)} %get-tuple-element.33.refs_0_, ...), custom_call_target="tpu_custom_call" | custom-call | tf_op jit(solution)/shard_map/store/pallas_call | solution.py:994
